TPU v7x, 256 devices: a 4x2x16 block of a 4x16x16 slice. The times are simulated.
256 devices in a mesh: grp: 2 (over y), sp: 16 (over z), fs: 4 (over x), tp: 2 (over core).
Axes of the slice: x: 4, y: 2, z: 16, core: 2. Of those that a mesh axis runs over, the one named last changes fastest.
The devices are a block of a 4x16x16 slice.
Arguments:
- tokens: bfloat16 [8, 8192, 2048], P(('grp', 'fs'), ('sp', 'tp')), parts along dimension 0, may hold values from -6 to 6
- norm_gain: float32 [2048], replicated, may hold values from 0.1 to 1.9
- w_bgate: bfloat16 [2048, 2048], P(('sp', 'fs'), 'tp'), may hold values from -0.125 to 0.125
- w_cgate: bfloat16 [2048, 2048], P(('sp', 'fs'), 'tp'), may hold values from -0.125 to 0.125
- w_conv_in: bfloat16 [2048, 2048], P(('sp', 'fs'), 'tp'), may hold values from -0.125 to 0.125
- conv_taps: bfloat16 [3, 2048], P(None, 'tp'), may hold values from -3.5 to 3.5
- w_query: bfloat16 [2048, 2048], P(('sp', 'fs'), 'tp'), may hold values from -0.13258252 to 0.13258252
- w_key: bfloat16 [2048, 256], P(('sp', 'fs'), 'tp'), may hold values from -4.02167 to 4.02167
- w_value: bfloat16 [2048, 256], P(('sp', 'fs'), 'tp'), may hold values from -0.125 to 0.125
- sink_logits: float32 [32], P('tp'), may hold values from 1 to 6
- conv_out_weight: bfloat16 [2048, 2048], P('tp', ('sp', 'fs')), may hold values from -0.125 to 0.125
- attn_out_weight: bfloat16 [2048, 2048], P('tp', ('sp', 'fs')), may hold values from -0.75 to 0.75
Outputs:
- mixed: bfloat16 [8, 8192, 2048], P(('grp', 'fs'), ('sp', 'tp')), parts along dimension 0
There are 2 independent parts, one for each index of `grp`. A program takes and returns all parts, laid end to end along the dimension named above; an argument that names none is the same for every part. Nothing has to cross between parts.
All inputs are finite; a program needn't handle non-finite values.
Results may differ from a plain program's by a relative error of at most 0.014.
The roundings to bfloat16 on the way count: a program that leaves them out, or rounds other values in their place, can miss the bound.
Values may be sent and summed in bfloat16 or wider, within the bound.
A program may use at most 128 MiB of HBM per device.

v0:
```python
import jax
import jax.numpy as jnp
from jax import lax
from jax.sharding import PartitionSpec as P

HEAD = 64
WINDOW = 128
TAPS = 3


epsilon = 1e-06


def joined_along(blocks, dim):
    lengths = list(blocks.shape[1:])
    lengths[dim] *= blocks.shape[0]
    return jnp.moveaxis(blocks, 0, dim).reshape(lengths)


def from_everyone(array, axis):
    copies = jnp.broadcast_to(array, (lax.axis_size(axis), *array.shape))
    return lax.all_to_all(copies, axis, split_axis=0, concat_axis=0, tiled=True)


def collect(array, axis, dim):
    return joined_along(from_everyone(array, axis), dim)


def in_one_piece(arrays, axis, dim, along):
    widths = [a.shape[along] for a in arrays]
    both = jnp.concatenate(arrays, axis=along)
    whole = lax.all_gather(both, axis, axis=dim, tiled=True)
    return tuple(jnp.split(whole, [sum(widths[:k]) for k in range(1, len(widths))], axis=along))


def shortened(array):

    def short(part):
        return part.astype(jnp.bfloat16) if part.dtype == jnp.float32 else part

    return jax.tree.map(short, array)


def shifted(array, axis, by):
    size = lax.axis_size(axis)
    pairs = [(i, i + by) for i in range(size) if 0 <= i + by < size]
    return lax.ppermute(array, axis, pairs)


def rows_first(arrays, axis, dims):
    turned = [jnp.moveaxis(a, dim, 0) for a, dim in zip(arrays, dims)]
    widths = [t[0].size for t in turned]
    both = jnp.concatenate([t.reshape(-1, w) for t, w in zip(turned, widths)], axis=1)
    whole = lax.all_gather(both, axis, axis=0, tiled=True)
    blocks = jnp.split(whole, [sum(widths[:k]) for k in range(1, len(widths))], axis=1)
    return tuple(
        (
            jnp.moveaxis(b.reshape(-1, *t.shape[1:]), 0, dim)
            for b, t, dim in zip(blocks, turned, dims)
        )
    )


def in_blocks(array, dim, size):
    lengths = array.shape
    blocks = array.reshape(*lengths[:dim], size, lengths[dim] // size, *lengths[dim + 1 :])
    return jnp.moveaxis(blocks, dim, 0)


def summed_on_arrival(array, axis, dim):
    size = lax.axis_size(axis)
    blocks = lax.all_to_all(in_blocks(array, dim, size), axis, 0, 0, tiled=True)
    return jnp.sum(blocks.astype(jnp.float32), axis=0)


def attend(queries, key_rows, value_rows, prev_keys, prev_values, sink_row, offset):
    length_here = queries.shape[0]
    kv_local = key_rows.shape[1] // HEAD
    heads_local = queries.shape[1] // HEAD
    groups = heads_local // kv_local
    blocks = length_here // WINDOW
    key_all = jnp.concatenate([prev_keys, key_rows], 0)
    value_all = jnp.concatenate([prev_values, value_rows], 0)
    key_band = jnp.concatenate(
        [
            key_all[:length_here].reshape(blocks, WINDOW, kv_local, HEAD),
            key_rows.reshape(blocks, WINDOW, kv_local, HEAD),
        ],
        1,
    )
    value_band = jnp.concatenate(
        [
            value_all[:length_here].reshape(blocks, WINDOW, kv_local, HEAD),
            value_rows.reshape(blocks, WINDOW, kv_local, HEAD),
        ],
        1,
    )
    query_blocks = queries.reshape(blocks, WINDOW, kv_local, groups, HEAD)
    scores = jnp.einsum(
        "nqhgd,nkhd->nhgqk", query_blocks, key_band, preferred_element_type=jnp.float32
    ) / jnp.sqrt(jnp.float32(HEAD))
    block_ids = jnp.arange(blocks)[:, None, None]
    query_pos = block_ids * WINDOW + jnp.arange(WINDOW)[None, :, None]
    key_pos = (block_ids - 1) * WINDOW + jnp.arange(2 * WINDOW)[None, None, :]
    allowed = (key_pos + offset >= 0) & (key_pos <= query_pos) & (query_pos - key_pos < WINDOW)
    scores = jnp.where(allowed[:, None, None], scores, -jnp.inf)
    sink_grid = sink_row.reshape(1, kv_local, groups, 1, 1)
    peak_score = jnp.maximum(jnp.max(scores, axis=-1, keepdims=True), sink_grid)
    weights = jnp.exp(scores - peak_score)
    denominator = jnp.sum(weights, axis=-1, keepdims=True) + jnp.exp(sink_grid - peak_score)
    probabilities = (weights / denominator).astype(jnp.bfloat16)
    attended = jnp.einsum(
        "nhgqk,nkhd->nqhgd", probabilities, value_band, preferred_element_type=jnp.float32
    )
    return attended.astype(jnp.bfloat16).reshape(length_here, heads_local * HEAD)


def project_all(features, weights):
    return tuple(
        (
            jnp.dot(features, weight, preferred_element_type=jnp.float32).astype(jnp.bfloat16)
            for weight in weights
        )
    )


def local(
    tokens,
    norm_gain,
    w_bgate,
    w_cgate,
    w_conv_in,
    conv_taps,
    w_query,
    w_key,
    w_value,
    sink_logits,
    conv_out_weight,
    attn_out_weight,
):
    widened = tokens[0].astype(jnp.float32)
    normed = (
        widened
        * lax.rsqrt(jnp.mean(widened * widened, axis=-1, keepdims=True) + epsilon)
        * norm_gain
    ).astype(jnp.bfloat16)
    in_weights = (w_bgate, w_cgate, w_conv_in, w_query, w_key, w_value)
    narrowed = (
        lax.all_to_all(in_weights[0], "fs", split_axis=1, concat_axis=0, tiled=True),
        lax.all_to_all(in_weights[1], "fs", split_axis=1, concat_axis=0, tiled=True),
        lax.all_to_all(in_weights[2], "fs", split_axis=1, concat_axis=0, tiled=True),
        lax.all_to_all(in_weights[3], "fs", split_axis=1, concat_axis=0, tiled=True),
        lax.all_to_all(in_weights[4], "fs", split_axis=1, concat_axis=0, tiled=True),
        lax.all_to_all(in_weights[5], "fs", split_axis=1, concat_axis=0, tiled=True),
    )
    everyone = collect(normed, ("fs", "tp"), 0)
    whole_columns = in_one_piece(
        (narrowed[0], narrowed[1], narrowed[2], narrowed[3], narrowed[4], narrowed[5]), "sp", 0, 1
    )
    rounded = project_all(everyone, whole_columns)
    projected = jax.tree.map(
        lambda part, own: part.astype(own.dtype),
        lax.all_to_all(shortened(rounded), "fs", split_axis=0, concat_axis=1, tiled=True),
        rounded,
    )
    out_gate, in_gate, conv_input, queries, key_rows, value_rows = projected
    length_here = queries.shape[0]
    gated = (in_gate.astype(jnp.float32) * conv_input.astype(jnp.float32)).astype(jnp.bfloat16)
    earlier = shifted(
        (
            gated[length_here - (TAPS - 1) :],
            key_rows[length_here - WINDOW :],
            value_rows[length_here - WINDOW :],
        ),
        "sp",
        1,
    )
    padded = jnp.concatenate([earlier[0], gated], 0)
    taps_wide = conv_taps.astype(jnp.float32)
    convolved = padded[0:length_here].astype(jnp.float32) * taps_wide[0]
    for which in range(1, TAPS):
        convolved = (
            convolved + padded[which : which + length_here].astype(jnp.float32) * taps_wide[which]
        )
    conv_branch = (out_gate.astype(jnp.float32) * convolved).astype(jnp.bfloat16)
    offset = lax.axis_index("sp") * length_here
    attended = attend(queries, key_rows, value_rows, earlier[1], earlier[2], sink_logits, offset)
    out_columns = rows_first((conv_out_weight, attn_out_weight), ("sp", "fs"), (1, 1))
    product = jnp.dot(conv_branch, out_columns[0], preferred_element_type=jnp.float32)
    summed = summed_on_arrival(
        (product + jnp.dot(attended, out_columns[1], preferred_element_type=jnp.float32)).astype(
            jnp.bfloat16
        ),
        "tp",
        0,
    )
    return summed.astype(jnp.bfloat16)[None]


def solution(mesh):
    placed = (
        P(("grp", "fs"), ("sp", "tp"), None),
        P(),
        P(("sp", "fs"), "tp"),
        P(("sp", "fs"), "tp"),
        P(("sp", "fs"), "tp"),
        P(None, "tp"),
        P(("sp", "fs"), "tp"),
        P(("sp", "fs"), "tp"),
        P(("sp", "fs"), "tp"),
        P("tp"),
        P("tp", ("sp", "fs")),
        P("tp", ("sp", "fs")),
    )
    return jax.shard_map(
        local,
        mesh=mesh,
        in_specs=placed,
        out_specs=P(("grp", "fs"), ("sp", "tp"), None),
        check_vma=False,
    )
```

profile of v0, /device:TPU:33, one launch (start us, length us, event | category | flops | bytes accessed | tf_op | source)
XLA Modules:
  0.0 342.4 jit_solution(8857954702506080556)
XLA Ops:
  8.2 5.1 %all-to-all-start.5 = ((bf16[4,2,512]{2,1,0:T(2,128)(2,1)}), bf16[4,2,512]{2,1,0:T(2,128)(2,1)S(1)}, u32[]{:S(2)}, u32[]{:S(2)}) async-start(bf16[4,2,512]{2,1,0:T(2,128)(2,1)} %reshape.196), calls=%async_computation.5 | async-start | bytes 16384 | tf_op jit(solution)/shard_map/all_to_all | solution.py:153
  14.8 2.7 all-to-all-done.5
  17.4 3.3 all-to-all-start.6
  22.2 2.6 all-to-all-done.6
  24.8 3.4 all-to-all-start.4
  29.7 2.9 all-to-all-done.4
  32.6 3.4 all-to-all-start.1
  40.4 3.4 all-to-all-start.2
  43.9 4.3 %all-to-all-done.2 = bf16[32,4,256]{2,0,1:T(8,128)(2,1)S(1)} async-done(((bf16[32,4,256]{2,0,1:T(8,128)(2,1)}), bf16[32,4,256]{2,0,1:T(8,128)(2,1)S(1)}, u32[]{:S(2)}, u32[]{:S(2)}) %all-to-all-start.2) | async-done | bytes 65568 | tf_op jit(solution)/shard_map/all_to_all | solution.py:150
  48.1 3.4 all-to-all-start.3
  51.8 4.1 %all-to-all-done.3 = bf16[32,4,256]{2,0,1:T(8,128)(2,1)S(1)} async-done(((bf16[32,4,256]{2,0,1:T(8,128)(2,1)}), bf16[32,4,256]{2,0,1:T(8,128)(2,1)S(1)}, u32[]{:S(2)}, u32[]{:S(2)}) %all-to-all-start.3) | async-done | bytes 65568 | tf_op jit(solution)/shard_map/all_to_all | solution.py:151
  56.8 1.5 pad_maximum_fusion.3
  61.0 4.3 %broadcast_in_dim.16 = bf16[8,256,2048]{2,1,0:T(8,128)(2,1)} broadcast(bf16[256,2048]{1,0:T(8,128)(2,1)S(1)} %fusion.11), dimensions={1,2} | broadcast | bytes 9437184 | tf_op jit(solution)/shard_map/broadcast_in_dim | solution.py:21
  65.3 30.3 %all-to-all-start = ((bf16[8,256,2048]{2,1,0:T(8,128)(2,1)}), bf16[8,256,2048]{2,1,0:T(8,128)(2,1)}, u32[]{:S(2)}, u32[]{:S(2)}) async-start(bf16[8,256,2048]{2,1,0:T(8,128)(2,1)} %broadcast_in_dim.16), calls=%async_computation | async-start | bytes 16777216 | tf_op jit(solution)/shard_map/all_to_all | solution.py:22
  95.9 95.5 %all-to-all-done = bf16[8,256,2048]{2,1,0:T(8,128)(2,1)} async-done(((bf16[8,256,2048]{2,1,0:T(8,128)(2,1)}), bf16[8,256,2048]{2,1,0:T(8,128)(2,1)}, u32[]{:S(2)}, u32[]{:S(2)}) %all-to-all-start) | async-done | bytes 8388640 | tf_op jit(solution)/shard_map/all_to_all | solution.py:22
  191.4 6.0 %convolution_convert_fusion.4 = bf16[2048,32]{0,1:T(8,128)(2,1)S(1)} fusion(bf16[2048,2048]{1,0:T(8,128)(2,1)} %bitcast.2, bf16[2048,1088]{1,0:T(8,128)(2,1)} %all-gather.3.cloned.1.call-done), kind=kOutput, calls=%fused_computation.17 | convolution fusion | flops 268500992 | bytes 9043968 | tf_op jit(solution)/shard_map/dot_general | solution.py:121
  198.1 3.4 all-to-all-start.11
  201.5 6.1 %convolution_convert_fusion.5 = bf16[2048,32]{0,1:T(8,128)(2,1)S(1)} fusion(bf16[2048,2048]{1,0:T(8,128)(2,1)} %bitcast.2, bf16[2048,1088]{1,0:T(8,128)(2,1)} %all-gather.3.cloned.1.call-done), kind=kOutput, calls=%fused_computation.18 | convolution fusion | flops 268500992 | bytes 9043968 | tf_op jit(solution)/shard_map/dot_general | solution.py:121
  208.3 4.1 %all-to-all-start.10 = ((bf16[4,512,32]{1,2,0:T(8,128)(2,1)}), bf16[4,512,32]{1,2,0:T(8,128)(2,1)S(1)}, u32[]{:S(2)}, u32[]{:S(2)}) async-start(bf16[4,512,32]{1,2,0:T(8,128)(2,1)} %bitcast.131), calls=%async_computation.10 | async-start | bytes 262144 | tf_op jit(solution)/shard_map/all_to_all | solution.py:163
  212.4 6.0 %convolution_convert_fusion = bf16[2048,256]{1,0:T(8,128)(2,1)S(1)} fusion(bf16[2048,2048]{1,0:T(8,128)(2,1)} %bitcast.2, bf16[2048,1088]{1,0:T(8,128)(2,1)} %all-gather.3.cloned.1.call-done), kind=kOutput, calls=%fused_computation.13 | convolution fusion | flops 2148007936 | bytes 10485760 | tf_op jit(solution)/shard_map/dot_general | solution.py:121
  219.7 4.3 %all-to-all-start.12 = ((bf16[4,512,256]{1,2,0:T(8,128)(2,1)}), bf16[4,512,256]{1,2,0:T(8,128)(2,1)S(1)}, u32[]{:S(2)}, u32[]{:S(2)}) async-start(bf16[4,512,256]{1,2,0:T(8,128)(2,1)} %copy.71), calls=%async_computation.12 | async-start | bytes 2097152 | tf_op jit(solution)/shard_map/all_to_all | solution.py:163
  224.3 6.0 %convolution_convert_fusion.2 = bf16[2048,256]{1,0:T(8,128)(2,1)S(1)} fusion(bf16[2048,2048]{1,0:T(8,128)(2,1)} %bitcast.2, bf16[2048,1088]{1,0:T(8,128)(2,1)} %all-gather.3.cloned.1.call-done), kind=kOutput, calls=%fused_computation.15 | convolution fusion | flops 2148007936 | bytes 10485760 | tf_op jit(solution)/shard_map/dot_general | solution.py:121
  231.6 5.3 %all-to-all-done.12 = bf16[4,512,256]{1,2,0:T(8,128)(2,1)S(1)} async-done(((bf16[4,512,256]{1,2,0:T(8,128)(2,1)}), bf16[4,512,256]{1,2,0:T(8,128)(2,1)S(1)}, u32[]{:S(2)}, u32[]{:S(2)}) %all-to-all-start.12) | async-done | bytes 1048608 | tf_op jit(solution)/shard_map/all_to_all | solution.py:163
  236.9 3.6 %all-to-all-start.8 = ((bf16[4,512,256]{1,2,0:T(8,128)(2,1)}), bf16[4,512,256]{1,2,0:T(8,128)(2,1)S(1)}, u32[]{:S(2)}, u32[]{:S(2)}) async-start(bf16[4,512,256]{1,2,0:T(8,128)(2,1)} %copy.63), calls=%async_computation.8 | async-start | bytes 2097152 | tf_op jit(solution)/shard_map/all_to_all | solution.py:163
  240.7 6.0 %convolution_convert_fusion.1 = bf16[2048,256]{1,0:T(8,128)(2,1)S(1)} fusion(bf16[2048,2048]{1,0:T(8,128)(2,1)} %bitcast.2, bf16[2048,1088]{1,0:T(8,128)(2,1)} %all-gather.3.cloned.1.call-done), kind=kOutput, calls=%fused_computation.14 | convolution fusion | flops 2148007936 | bytes 10485760 | tf_op jit(solution)/shard_map/dot_general | solution.py:121
  248.6 1.9 collective-permute-start.2
  250.5 14.8 %all-to-all-done.8 = bf16[4,512,256]{1,2,0:T(8,128)(2,1)S(1)} async-done(((bf16[4,512,256]{1,2,0:T(8,128)(2,1)}), bf16[4,512,256]{1,2,0:T(8,128)(2,1)S(1)}, u32[]{:S(2)}, u32[]{:S(2)}) %all-to-all-start.8) | async-done | bytes 1048608 | tf_op jit(solution)/shard_map/all_to_all | solution.py:163
  265.3 3.6 %all-to-all-start.9 = ((bf16[4,512,256]{1,2,0:T(8,128)(2,1)}), bf16[4,512,256]{1,2,0:T(8,128)(2,1)S(1)}, u32[]{:S(2)}, u32[]{:S(2)}) async-start(bf16[4,512,256]{1,2,0:T(8,128)(2,1)} %copy.64), calls=%async_computation.9 | async-start | bytes 2097152 | tf_op jit(solution)/shard_map/all_to_all | solution.py:163
  269.0 7.0 %convolution_convert_fusion.3 = bf16[2048,256]{1,0:T(8,128)(2,1)} fusion(bf16[2048,2048]{1,0:T(8,128)(2,1)} %bitcast.2, bf16[2048,1088]{1,0:T(8,128)(2,1)} %all-gather.3.cloned.1.call-done), kind=kOutput, calls=%fused_computation.16 | convolution fusion | flops 2148007936 | bytes 10485760 | tf_op jit(solution)/shard_map/dot_general | solution.py:121
  276.0 2.3 copy.62
  280.3 1.6 copy.70
  281.8 1.9 collective-permute-start.1
  283.7 1.6 copy.67
  286.7 1.6 reshape.187
  288.4 1.6 copy.69
  291.4 1.6 reshape.185
  293.0 1.6 copy.66
  295.6 4.4 %all-to-all-start.7 = ((bf16[4,512,256]{1,2,0:T(8,128)(2,1)}), bf16[4,512,256]{1,2,0:T(8,128)(2,1)}, u32[]{:S(2)}, u32[]{:S(2)}) async-start(bf16[4,512,256]{1,2,0:T(8,128)(2,1)} %copy.62), calls=%async_computation.7 | async-start | bytes 2097152 | tf_op jit(solution)/shard_map/all_to_all | solution.py:163
  301.1 2.0 collective-permute-start
  303.2 2.5 fusion.1
  305.8 2.4 fusion
  308.3 2.4 fusion.14
  311.9 3.0 fusion.12
  314.9 1.9 all-gather.5.cloned.1.call-done
  316.7 4.7 %fusion.2 = f32[512,2048]{1,0:T(8,128)S(1)} fusion(bf16[2048,2048]{1,0:T(8,128)(2,1)} %all-gather.5.cloned.1.call-done, bf16[128,8,4,128]{3,2,1,0:T(4,128)(2,1)S(1)} %bitcast.146), kind=kOutput, calls=%fused_computation.5 | convolution fusion | flops 2147483648 | bytes 9437184 | tf_op jit(solution)/shard_map/dot_general | solution.py:191
  321.5 2.4 add_convert_fusion
  323.9 10.0 %all_to_all.217 = bf16[2,256,2048]{2,1,0:T(8,128)(2,1)S(1)} all-to-all(bf16[2,256,2048]{2,1,0:T(8,128)(2,1)S(1)} %bitcast.139), channel_id=1, replica_groups=mesh['grp'=2,'sp'=16,'fs'=4,'tp'=2] {'tp'}, dimensions={0} | all-to-all | bytes 4194304 | tf_op jit(solution)/shard_map/all_to_all | solution.py:72
  333.8 1.7 reduce_sum.32
  (72 shorter events, 29.3 us)
Async XLA Ops:
  6.5 53.4 %copy-start = (bf16[1,256,2048]{2,1,0:T(8,128)(2,1)S(1)}, bf16[1,256,2048]{2,1,0:T(8,128)(2,1)}, u32[]{:S(2)}) copy-start(bf16[1,256,2048]{2,1,0:T(8,128)(2,1)} %param.12) | copy-start | bytes 3145732
  8.2 9.3 %all-to-all-start.5 = ((bf16[4,2,512]{2,1,0:T(2,128)(2,1)}), bf16[4,2,512]{2,1,0:T(2,128)(2,1)S(1)}, u32[]{:S(2)}, u32[]{:S(2)}) async-start(bf16[4,2,512]{2,1,0:T(2,128)(2,1)} %reshape.196), calls=%async_computation.5 | async-start | bytes 16384 | tf_op jit(solution)/shard_map/all_to_all | solution.py:153
  17.4 7.4 %all-to-all-start.6 = ((bf16[4,2,512]{2,1,0:T(2,128)(2,1)}), bf16[4,2,512]{2,1,0:T(2,128)(2,1)S(1)}, u32[]{:S(2)}, u32[]{:S(2)}) async-start(bf16[4,2,512]{2,1,0:T(2,128)(2,1)} %reshape.198), calls=%async_computation.6 | async-start | bytes 16384 | tf_op jit(solution)/shard_map/all_to_all | solution.py:154
  24.8 7.8 %all-to-all-start.4 = ((bf16[32,4,256]{2,0,1:T(8,128)(2,1)}), bf16[32,4,256]{2,0,1:T(8,128)(2,1)S(1)}, u32[]{:S(2)}, u32[]{:S(2)}) async-start(bf16[32,4,256]{2,0,1:T(8,128)(2,1)} %bitcast.132), calls=%async_computation.4 | async-start | bytes 131072 | tf_op jit(solution)/shard_map/all_to_all | solution.py:152
  32.6 7.8 %all-to-all-start.1 = ((bf16[32,4,256]{2,0,1:T(8,128)(2,1)}), bf16[32,4,256]{2,0,1:T(8,128)(2,1)S(1)}, u32[]{:S(2)}, u32[]{:S(2)}) async-start(bf16[32,4,256]{2,0,1:T(8,128)(2,1)} %bitcast.135), calls=%async_computation.1 | async-start | bytes 131072 | tf_op jit(solution)/shard_map/all_to_all | solution.py:149
  40.4 7.8 %all-to-all-start.2 = ((bf16[32,4,256]{2,0,1:T(8,128)(2,1)}), bf16[32,4,256]{2,0,1:T(8,128)(2,1)S(1)}, u32[]{:S(2)}, u32[]{:S(2)}) async-start(bf16[32,4,256]{2,0,1:T(8,128)(2,1)} %bitcast.134), calls=%async_computation.2 | async-start | bytes 131072 | tf_op jit(solution)/shard_map/all_to_all | solution.py:150
  48.1 7.8 %all-to-all-start.3 = ((bf16[32,4,256]{2,0,1:T(8,128)(2,1)}), bf16[32,4,256]{2,0,1:T(8,128)(2,1)S(1)}, u32[]{:S(2)}, u32[]{:S(2)}) async-start(bf16[32,4,256]{2,0,1:T(8,128)(2,1)} %bitcast.133), calls=%async_computation.3 | async-start | bytes 131072 | tf_op jit(solution)/shard_map/all_to_all | solution.py:151
  51.5 139.9 %all-gather.3.cloned.1.call-start = ((), (), s32[]{:S(2)}) async-start(), calls=%async_computation.14 | async-start | bytes 5013504 | tf_op jit(solution)/shard_map/all_gather | solution.py:32
  56.8 260.0 %all-gather.5.cloned.1.call-start = ((), (), s32[]{:S(2)}) async-start(), calls=%async_computation.15 | async-start | bytes 8519680 | tf_op jit(solution)/shard_map/all_gather | solution.py:54
  65.3 126.1 %all-to-all-start = ((bf16[8,256,2048]{2,1,0:T(8,128)(2,1)}), bf16[8,256,2048]{2,1,0:T(8,128)(2,1)}, u32[]{:S(2)}, u32[]{:S(2)}) async-start(bf16[8,256,2048]{2,1,0:T(8,128)(2,1)} %broadcast_in_dim.16), calls=%async_computation | async-start | bytes 16777216 | tf_op jit(solution)/shard_map/all_to_all | solution.py:22
  198.1 10.2 %all-to-all-start.11 = ((bf16[4,512,32]{1,2,0:T(8,128)(2,1)}), bf16[4,512,32]{1,2,0:T(8,128)(2,1)S(1)}, u32[]{:S(2)}, u32[]{:S(2)}) async-start(bf16[4,512,32]{1,2,0:T(8,128)(2,1)} %bitcast.130), calls=%async_computation.11 | async-start | bytes 262144 | tf_op jit(solution)/shard_map/all_to_all | solution.py:163
  208.3 11.4 %all-to-all-start.10 = ((bf16[4,512,32]{1,2,0:T(8,128)(2,1)}), bf16[4,512,32]{1,2,0:T(8,128)(2,1)S(1)}, u32[]{:S(2)}, u32[]{:S(2)}) async-start(bf16[4,512,32]{1,2,0:T(8,128)(2,1)} %bitcast.131), calls=%async_computation.10 | async-start | bytes 262144 | tf_op jit(solution)/shard_map/all_to_all | solution.py:163
  219.7 17.2 %all-to-all-start.12 = ((bf16[4,512,256]{1,2,0:T(8,128)(2,1)}), bf16[4,512,256]{1,2,0:T(8,128)(2,1)S(1)}, u32[]{:S(2)}, u32[]{:S(2)}) async-start(bf16[4,512,256]{1,2,0:T(8,128)(2,1)} %copy.71), calls=%async_computation.12 | async-start | bytes 2097152 | tf_op jit(solution)/shard_map/all_to_all | solution.py:163
  224.3 16.2 %copy-start.5 = (bf16[3,1024]{1,0:T(4,128)(2,1)S(1)}, bf16[3,1024]{1,0:T(4,128)(2,1)}, u32[]{:S(2)}) copy-start(bf16[3,1024]{1,0:T(4,128)(2,1)} %param.17) | copy-start | bytes 18436
  224.3 16.2 %copy-start.7 = (f32[16]{0:T(128)S(1)}, f32[16]{0:T(128)}, u32[]{:S(2)}) copy-start(f32[16]{0:T(128)} %param.21) | copy-start | bytes 196
  236.9 28.4 %all-to-all-start.8 = ((bf16[4,512,256]{1,2,0:T(8,128)(2,1)}), bf16[4,512,256]{1,2,0:T(8,128)(2,1)S(1)}, u32[]{:S(2)}, u32[]{:S(2)}) async-start(bf16[4,512,256]{1,2,0:T(8,128)(2,1)} %copy.63), calls=%async_computation.8 | async-start | bytes 2097152 | tf_op jit(solution)/shard_map/all_to_all | solution.py:163
  248.6 36.7 %collective-permute-start.2 = (bf16[128,128]{0,1:T(8,128)(2,1)}, bf16[128,128]{0,1:T(8,128)(2,1)}, u32[]{:S(2)}, u32[]{:S(2)}) collective-permute-start(bf16[128,128]{0,1:T(8,128)(2,1)} %bitcast.37), channel_id=1, source_target_pairs={{0,8},{8,16},{16,24},{24,32},{32,40},{40,48},{48,56},{56,64},{64,7... | collective-permute-start | bytes 98312 | tf_op jit(solution)/shard_map/ppermute | solution.py:47
  265.3 30.3 %all-to-all-start.9 = ((bf16[4,512,256]{1,2,0:T(8,128)(2,1)}), bf16[4,512,256]{1,2,0:T(8,128)(2,1)S(1)}, u32[]{:S(2)}, u32[]{:S(2)}) async-start(bf16[4,512,256]{1,2,0:T(8,128)(2,1)} %copy.64), calls=%async_computation.9 | async-start | bytes 2097152 | tf_op jit(solution)/shard_map/all_to_all | solution.py:163
  281.8 8.1 %collective-permute-start.1 = (bf16[128,128]{0,1:T(8,128)(2,1)}, bf16[128,128]{0,1:T(8,128)(2,1)}, u32[]{:S(2)}, u32[]{:S(2)}) collective-permute-start(bf16[128,128]{0,1:T(8,128)(2,1)} %bitcast.167), channel_id=1, source_target_pairs={{0,8},{8,16},{16,24},{24,32},{32,40},{40,48},{48,56},{56,64},{64,7... | collective-permute-start | bytes 98312 | tf_op jit(solution)/shard_map/ppermute | solution.py:47
  286.7 16.4 %copy-start.1 = (bf16[4,128,2,64]{1,3,2,0:T(8,128)(2,1)S(1)}, bf16[4,128,2,64]{1,3,2,0:T(8,128)(2,1)}, u32[]{:S(2)}) copy-start(bf16[4,128,2,64]{1,3,2,0:T(8,128)(2,1)} %copy.70) | copy-start | bytes 393220
  291.4 11.8 %copy-start.2 = (bf16[4,128,2,64]{1,3,2,0:T(8,128)(2,1)S(1)}, bf16[4,128,2,64]{1,3,2,0:T(8,128)(2,1)}, u32[]{:S(2)}) copy-start(bf16[4,128,2,64]{1,3,2,0:T(8,128)(2,1)} %copy.69) | copy-start | bytes 393220
  295.6 15.9 %all-to-all-start.7 = ((bf16[4,512,256]{1,2,0:T(8,128)(2,1)}), bf16[4,512,256]{1,2,0:T(8,128)(2,1)}, u32[]{:S(2)}, u32[]{:S(2)}) async-start(bf16[4,512,256]{1,2,0:T(8,128)(2,1)} %copy.62), calls=%async_computation.7 | async-start | bytes 2097152 | tf_op jit(solution)/shard_map/all_to_all | solution.py:163
  301.1 10.8 %collective-permute-start = (bf16[2,1024]{0,1:T(8,128)(2,1)}, bf16[2,1024]{0,1:T(8,128)(2,1)}, u32[]{:S(2)}, u32[]{:S(2)}) collective-permute-start(bf16[2,1024]{0,1:T(8,128)(2,1)} %bitcast.23), channel_id=1, source_target_pairs={{0,8},{8,16},{16,24},{24,32},{32,40},{40,48},{48,56},{56,64},{64,7... | collective-permute-start | bytes 12296 | tf_op jit(solution)/shard_map/ppermute | solution.py:47
  305.7 2.5 copy-start.3
  305.7 2.5 copy-start.4
  316.7 4.7 %copy-start.6 = (bf16[2048,2048]{1,0:T(8,128)(2,1)S(1)}, bf16[2048,2048]{1,0:T(8,128)(2,1)}, u32[]{:S(2)}) copy-start(bf16[2048,2048]{1,0:T(8,128)(2,1)} %all-gather.5.cloned.1.call-done) | copy-start | bytes 25165828
Sparse Core Ops, SparseCore 0:
  56.9 87.4 all-gather.2
  146.8 169.8 all-gather.4
where the time goes:
time: 344 us; the launch traced here: 342 us
  waiting for transfers between devices  136 us (40%)
  starting transfers between devices  81.6 us (24%)
  matrix products  49.1 us (14%)
  local copies, waits for them, and re-layouts  37.2 us (11%)
  other arithmetic  15 us (4%)
  between operations  13.7 us (4%)
  blocking collectives  9.96 us (3%)
    all_to_all x1, waiting for transfers between devices, from_everyone(): return lax.all_to_all(copies, axis, split_axis=0, concat_axis=0, tiled=True)  95.5 us
    dot_general x6, matrix products, project_all(): jnp.dot(features, weight, preferred_element_type=jnp.float32)  37.1 us
    all_to_all x1, starting transfers between devices, from_everyone(): return lax.all_to_all(copies, axis, split_axis=0, concat_axis=0, tiled=True)  30.3 us
    all_to_all x6, starting transfers between devices, local(): lax.all_to_all(shortened(rounded), 'fs', split_axis=0, concat_axis=1, til...  23.4 us
    all_to_all x6, waiting for transfers between devices, local(): lax.all_to_all(shortened(rounded), 'fs', split_axis=0, concat_axis=1, til...  20.1 us
    all_to_all x1, blocking collectives, summed_on_arrival(): blocks = lax.all_to_all(in_blocks(array, dim, size), axis, 0, 0, tiled=True)  9.96 us
    all_to_all x6, local copies, waits for them, and re-layouts, local(): lax.all_to_all(shortened(rounded), 'fs', split_axis=0, concat_axis=1, til...  7.65 us
  transfers between devices with their start and end apart: 18, of which 11 were waited for; matrix products, arithmetic and copies ran while one was open for 26% of the time, Pallas kernels for 0%

commit v1 on v0

v1 whole, which is shorter than its diff:
```python
import functools

import jax
import jax.numpy as jnp
from jax import lax
from jax.experimental import pallas as pl
from jax.experimental.pallas import tpu as pltpu
from jax.sharding import PartitionSpec as P

HEAD = 64
WINDOW = 128
TAPS = 3
EPSILON = 1e-06
MESH = pl.DeviceIdType.MESH
F32 = jnp.float32
BF16 = jnp.bfloat16
TILE = 256


def rows_dot(a, b):
    return lax.dot_general(a, b, (((1,), (1,)), ((), ())), preferred_element_type=F32)


def layer_kernel(
    ns,
    nf,
    xn,
    w_query,
    w_conv_in,
    w_cgate,
    w_bgate,
    kv_pack,
    out_pack,
    aux_in,
    out,
    x_all,
    w_in,
    w_out,
    proj,
    kv_rows,
    gated,
    acts,
    aux,
    send_far,
    recv_far,
    send_near,
    recv_near,
    own_sum,
    first_send,
    first_recv,
    z_send,
    z_recv,
    p_send,
    p_recv,
    x_send,
    x_recv,
    aux_send,
    aux_recv,
    halo_send,
    halo_recv,
    far_send,
    far_recv,
    near_send,
    near_recv,
):
    s = lax.axis_index("sp")
    f = lax.axis_index("fs")
    t = lax.axis_index("tp")
    s_next, s_prev = lax.rem(s + 1, ns), lax.rem(s + ns - 1, ns)
    f_next, f_prev = lax.rem(f + 1, nf), lax.rem(f + nf - 1, nf)
    f_far = lax.rem(f + 2, nf)
    other = 1 - t
    rows, width = xn.shape
    rb = w_query.shape[0]
    quarter = w_query.shape[1] // 2
    kvw = kv_pack.shape[2]
    half = rows // 2
    blocks = rows // WINDOW

    def remote(src, dst, send_sem, recv_sem, **where):
        return pltpu.make_async_remote_copy(
            src_ref=src,
            dst_ref=dst,
            send_sem=send_sem,
            recv_sem=recv_sem,
            device_id=where,
            device_id_type=MESH,
        )

    barrier = pltpu.get_barrier_semaphore()
    for df in range(nf):
        for dt in range(2):
            if df == 0 and dt == 0:
                continue
            pl.semaphore_signal(
                barrier,
                inc=1,
                device_id={"fs": lax.rem(f + df, nf), "tp": lax.rem(t + dt, 2)},
                device_id_type=MESH,
            )
    for neighbour in (s_next, s_prev):
        for dt in range(2):
            pl.semaphore_signal(
                barrier,
                inc=1,
                device_id={"sp": neighbour, "tp": lax.rem(t + dt, 2)},
                device_id_type=MESH,
            )
    pl.semaphore_wait(barrier, 2 * nf - 1 + 4)

    weights = (w_in, w_out)
    mine = f // 2
    for j in range(2):
        to_f = 2 * t + j
        sources = [w.at[:, pl.ds(j * quarter, quarter)] for w in (w_query, w_conv_in, w_cgate, w_bgate)]
        sources.append(kv_pack.at[j])
        spans = [pl.ds(n * quarter, quarter) for n in range(4)] + [pl.ds(4 * quarter, kvw)]
        slot = pl.ds(lax.rem(f, 2) * rb, rb)
        here = jnp.logical_and(to_f == f, mine == t)

        @pl.when(jnp.logical_not(here))
        def _():
            for src, span in zip(sources, spans):
                remote(
                    src,
                    w_in.at[s, mine, slot, span],
                    first_send.at[0, j],
                    first_recv.at[0, lax.rem(f, 2)],
                    fs=to_f,
                    tp=mine,
                ).start()
            remote(
                out_pack.at[j],
                w_out.at[s, mine, slot],
                first_send.at[1, j],
                first_recv.at[1, lax.rem(f, 2)],
                fs=to_f,
                tp=mine,
            ).start()

        @pl.when(here)
        def _():
            for src, span in zip(sources, spans):
                w_in[s, mine, slot, span] = src[...]
            w_out[s, mine, slot] = out_pack[j]

    remote(aux_in, aux.at[t], aux_send, aux_recv, tp=other).start()

    halves = (pl.ds(0, half), pl.ds(half, half))
    for which in (0, 1):
        remote(xn.at[halves[which]], x_all.at[f, halves[which]], x_send.at[0], x_recv.at[0, which], fs=f_next).start()
        remote(xn.at[halves[1 - which]], x_all.at[f, halves[1 - which]], x_send.at[1], x_recv.at[1, 1 - which], fs=f_prev).start()
    x_all[f] = xn[...]
    aux[t] = aux_in[...]

    def wait_first(k):
        for i in range(2):
            local = jnp.logical_and(t == f // 2, f == 2 * t + i)

            @pl.when(jnp.logical_not(local))
            def _():
                piece = weights[k].at[s, t, pl.ds(i * rb, rb)]
                remote(piece, piece, first_send.at[k, 0], first_recv.at[k, i], tp=other).wait_recv()

    reach = ((ns // 2, ns // 2 - 1), (ns // 2 - 1, ns // 2))

    def onward(k, slot, i, way, hop):
        piece = weights[k].at[slot, t, pl.ds(i * rb, rb)]
        return remote(
            piece, piece, z_send.at[k, way], z_recv.at[k, way, i, hop], sp=(s_next, s_prev)[way]
        )

    def across(k, slot, i):
        piece = weights[k].at[slot, t, pl.ds(i * rb, rb)]
        return remote(piece, piece, p_send.at[k], p_recv.at[k], tp=other)

    def launch(k):
        for i in range(2):
            for way in range(2):
                if reach[way][i] >= 1:
                    onward(k, s, i, way, 1).start()
        for i in range(2):
            across(k, s, i).start()

    def when(condition, body):
        if isinstance(condition, bool):
            if condition:
                body()
        else:
            pl.when(condition)(body)

    def ring_step(k, hop):
        for i in range(2):
            for way in range(2):
                slot = lax.rem(s + ns - hop, ns) if way == 0 else lax.rem(s + hop, ns)

                def body(slot=slot, i=i, way=way):
                    onward(k, slot, i, way, hop).wait_recv()
                    when(hop < reach[way][i], lambda: onward(k, slot, i, way, hop + 1).start())
                    across(k, slot, i).start()

                when(hop <= reach[way][i], body)

    def wait_across(k):
        piece = weights[k].at[:, other]
        remote(piece, piece, p_send.at[k], p_recv.at[k], tp=other).wait_recv()

    wait_first(0)
    launch(0)
    early = max(1, ns // 4)
    for hop in range(1, early):
        ring_step(0, hop)

    def x_block(which, part, way, kind):
        ref = x_all.at[which, halves[part]]
        return remote(ref, ref, x_send.at[way], x_recv.at[way, kind], fs=(f_next, f_prev)[way])

    x_block(f_prev, 0, 0, 0).wait_recv()
    x_block(f_prev, 0, 0, 2).start()
    x_block(f_next, 1, 1, 1).wait_recv()
    x_block(f_next, 1, 1, 2).start()
    for hop in range(early, ns // 2):
        ring_step(0, hop)
    wait_first(1)
    launch(1)
    ring_step(0, ns // 2)
    x_block(f_prev, 1, 0, 1).wait_recv()
    x_block(f_next, 0, 1, 0).wait_recv()
    x_block(f_far, 0, 0, 2).wait_recv()
    x_block(f_far, 1, 1, 2).wait_recv()
    wait_across(0)
    remote(aux_in, aux.at[other], aux_send, aux_recv, tp=other).wait_recv()

    def project(column, size):
        w = w_in[:, :, :, pl.ds(column, size)].reshape(width, size)
        a = x_all[...].reshape(nf * rows, width)
        return jnp.dot(a, w, preferred_element_type=F32).astype(BF16)

    kv_rows[:, WINDOW:, :] = project(4 * quarter, kvw).reshape(nf, rows, kvw)

    kv_src, kv_dst = kv_rows.at[:, pl.ds(rows, WINDOW)], kv_rows.at[:, pl.ds(0, WINDOW)]
    gated_src, gated_dst = gated.at[:, pl.ds(rows, 16)], gated.at[:, pl.ds(0, 16)]

    def send_halo(n, src, dst):
        @pl.when(t == 0)
        def _():
            remote(src, dst, halo_send.at[n], halo_recv.at[n], tp=1).start()

        @pl.when(t == 1)
        def _():
            remote(src, dst, halo_send.at[n], halo_recv.at[n], sp=s_next, tp=0).start()

    tiles = 4 * quarter // TILE

    def projection(n, carry):
        when(n < ns // 2, lambda: ring_step(1, n + 1))
        proj[n] = project(pl.multiple_of(n * TILE, TILE), TILE).reshape(nf, rows, TILE)
        return carry

    send_halo(0, kv_src, kv_dst)
    lax.fori_loop(0, tiles, projection, 0)
    for hop in range(tiles + 1, ns // 2 + 1):
        ring_step(1, hop)

    per = quarter // TILE

    def gate(q, carry):
        for n in range(per):
            g = proj[per + n, q].astype(F32) * proj[2 * per + n, q].astype(F32)
            gated[q, 16:, pl.ds(n * TILE, TILE)] = g.astype(BF16)
        return carry

    lax.fori_loop(0, nf, gate, 0)
    send_halo(1, gated_src, gated_dst)

    aux_here = aux.at[f // 2, lax.rem(f, 2)]
    at_start = jnp.logical_and(s == 0, t == 0)

    remote(kv_dst, kv_dst, halo_send.at[0], halo_recv.at[0], tp=other).wait_recv()
    key_id = lax.broadcasted_iota(jnp.int32, (WINDOW, 2 * WINDOW), 1)
    query_id = lax.broadcasted_iota(jnp.int32, (WINDOW, 2 * WINDOW), 0)
    low = lax.broadcasted_iota(jnp.int32, (2 * WINDOW, kvw), 1) < HEAD

    def attend(step, carry):
        q = step // blocks
        b = lax.rem(step, blocks)
        begin = pl.multiple_of(b * WINDOW, WINDOW)
        both = kv_rows[q, pl.ds(begin, 2 * WINDOW), :].astype(F32)
        turned = pltpu.roll(both, HEAD, 1)
        zero = jnp.zeros_like(both)
        keys = jnp.concatenate([jnp.where(low, both, zero), jnp.where(low, zero, turned)], 0).astype(BF16)
        values = jnp.concatenate([jnp.where(low, turned, zero), jnp.where(low, zero, both)], 0).astype(BF16)
        first_key = jnp.where(jnp.logical_and(at_start, b == 0), WINDOW, 0)
        allowed = (key_id > query_id) & (key_id <= query_id + WINDOW) & (key_id >= first_key)
        for pair in range(quarter // (2 * HEAD)):
            n, lane = pair * 2 * HEAD // TILE, pair * 2 * HEAD % TILE
            queries = proj[n, q, pl.ds(begin, WINDOW), lane : lane + 2 * HEAD]
            scores = rows_dot(queries, keys) * (1.0 / HEAD**0.5)
            probs = []
            for h in range(2):
                score = jnp.where(allowed, scores[:, h * 2 * WINDOW : (h + 1) * 2 * WINDOW], -jnp.inf)
                sink = aux_here[8 + 2 * pair + h : 9 + 2 * pair + h, 0:1]
                peak = jnp.maximum(jnp.max(score, axis=-1, keepdims=True), sink)
                weight = jnp.exp(score - peak)
                total = jnp.sum(weight, axis=-1, keepdims=True) + jnp.exp(sink - peak)
                probs.append((weight * (1.0 / total)).astype(BF16))
            attended = jnp.dot(jnp.concatenate(probs, 1), values, preferred_element_type=F32)
            acts[q, pl.ds(begin, WINDOW), quarter + pair * 2 * HEAD : quarter + (pair + 1) * 2 * HEAD] = attended.astype(BF16)
        return carry

    lax.fori_loop(0, nf * blocks, attend, 0)

    remote(gated_dst, gated_dst, halo_send.at[1], halo_recv.at[1], tp=other).wait_recv()

    @pl.when(at_start)
    def _():
        gated[:, 0:16, :] = jnp.zeros_like(gated[:, 0:16, :])

    def convolve(q, carry):
        for n in range(per):
            span = pl.ds(n * TILE, TILE)
            g = gated[q, :, span].astype(F32)
            taps = aux_here[0:TAPS, n * TILE : (n + 1) * TILE]
            total = pltpu.roll(g, 2, 0)[16:] * taps[0:1] + pltpu.roll(g, 1, 0)[16:] * taps[1:2] + g[16:] * taps[2:3]
            acts[q, :, span] = (proj[3 * per + n, q].astype(F32) * total).astype(BF16)
        return carry

    lax.fori_loop(0, nf, convolve, 0)

    wait_across(1)
    count = width // TILE
    near_half = count // 2
    chips = TILE // (2 * 2 * rb)

    def partial(q, n):
        w = w_out[pl.ds(n * chips, chips)].reshape(TILE, 2 * quarter)
        return rows_dot(acts[q], w)

    ways = ((f_next, f_prev), (f_prev, f_next))

    def far_copy(way, n):
        return remote(
            send_far.at[way, n], recv_far.at[way, n], far_send.at[way], far_recv.at[way, n], fs=ways[way][0]
        )

    def near_copy(way, n):
        return remote(
            send_near.at[way, n], recv_near.at[way, n], near_send.at[way], near_recv.at[way, n], fs=ways[way][0]
        )

    def far_step(n, carry):
        send_far[0, n] = partial(f_far, n).astype(BF16)
        send_far[1, n] = partial(f_far, n + near_half).astype(BF16)
        far_copy(0, n).start()
        far_copy(1, n).start()
        return carry

    def plain_step(n, carry):
        send_near[0, n + near_half] = partial(f_next, n + near_half).astype(BF16)
        send_near[1, n] = partial(f_prev, n).astype(BF16)
        near_copy(0, n + near_half).start()
        near_copy(1, n).start()
        return carry

    def joined_step(n, carry):
        first, second = partial(f_next, n), partial(f_prev, n + near_half)
        far_copy(0, n).wait_recv()
        far_copy(1, n).wait_recv()
        send_near[0, n] = (first + recv_far[0, n].astype(F32)).astype(BF16)
        send_near[1, n + near_half] = (second + recv_far[1, n].astype(F32)).astype(BF16)
        near_copy(0, n).start()
        near_copy(1, n + near_half).start()
        return carry

    def own_step(n, carry):
        own_sum[n] = partial(f, n)
        return carry

    lax.fori_loop(0, near_half, far_step, 0)
    lax.fori_loop(0, near_half, plain_step, 0)
    lax.fori_loop(0, near_half, joined_step, 0)
    lax.fori_loop(0, count, own_step, 0)
    for n in range(near_half):
        for way, tile in ((0, n + near_half), (1, n)):
            near_copy(way, tile).wait_recv()
    for n in range(near_half):
        for way, tile in ((0, n), (1, n + near_half)):
            near_copy(way, tile).wait_recv()
        for tile in (n, n + near_half):
            total = own_sum[tile] + recv_near[0, tile].astype(F32) + recv_near[1, tile].astype(F32)
            out[:, tile * TILE : (tile + 1) * TILE] = total.astype(BF16)

    for k in range(2):
        for j in range(2):
            here = jnp.logical_and(2 * t + j == f, mine == t)

            @pl.when(jnp.logical_not(here))
            def _():
                piece = weights[k].at[s, t, pl.ds(0, rb)]
                remote(piece, piece, first_send.at[k, j], first_recv.at[k, 0], tp=other).wait_send()

        for way in range(2):
            pieces = weights[k].at[pl.ds(0, ns - 1), 0, pl.ds(0, rb)]
            remote(pieces, pieces, z_send.at[k, way], z_recv.at[k, way, 0, 0], tp=other).wait_send()
        piece = weights[k].at[:, t]
        remote(piece, piece, p_send.at[k], p_recv.at[k], tp=other).wait_send()
    for way in range(2):
        ref = x_all.at[pl.ds(0, 3), halves[0]]
        remote(ref, ref, x_send.at[way], x_recv.at[way, 0], tp=other).wait_send()
        remote(send_far.at[way], send_far.at[way], far_send.at[way], far_recv.at[way, 0], tp=other).wait_send()
        remote(send_near.at[way], send_near.at[way], near_send.at[way], near_recv.at[way, 0], tp=other).wait_send()
    remote(aux_in, aux_in, aux_send, aux_recv, tp=other).wait_send()
    remote(kv_src, kv_src, halo_send.at[0], halo_recv.at[0], tp=other).wait_send()
    remote(gated_src, gated_src, halo_send.at[1], halo_recv.at[1], tp=other).wait_send()


def local(
    ns,
    nf,
    tokens,
    norm_gain,
    w_bgate,
    w_cgate,
    w_conv_in,
    conv_taps,
    w_query,
    w_key,
    w_value,
    sink_logits,
    conv_out_weight,
    attn_out_weight,
):
    widened = tokens[0].astype(F32)
    normed = (
        widened * lax.rsqrt(jnp.mean(widened * widened, axis=-1, keepdims=True) + EPSILON) * norm_gain
    ).astype(BF16)
    rows, width = normed.shape
    rb, columns = w_query.shape
    quarter = columns // 2
    kvw = w_key.shape[1]
    kv_pack = jnp.stack(
        [
            jnp.concatenate([w[:, j * HEAD : (j + 1) * HEAD] for w in (w_key, w_value)], axis=1)
            for j in range(2)
        ]
    )
    out_pack = jnp.concatenate(
        [jnp.swapaxes(w.reshape(2, quarter, rb), 1, 2) for w in (conv_out_weight, attn_out_weight)], axis=2
    )
    heads = quarter // HEAD
    taps = jnp.swapaxes(conv_taps.astype(F32).reshape(TAPS, 2, quarter), 0, 1)
    sinks = jnp.broadcast_to(sink_logits.reshape(2, heads, 1), (2, heads, quarter))
    aux = jnp.concatenate([jnp.pad(taps, ((0, 0), (0, 8 - TAPS), (0, 0))), sinks], axis=1)
    count = width // TILE
    vmem = pl.BlockSpec(memory_space=pltpu.VMEM)
    dma = pltpu.SemaphoreType.DMA
    inside = 4 * quarter + kvw
    out = pl.pallas_call(
        functools.partial(layer_kernel, ns, nf),
        out_shape=jax.ShapeDtypeStruct((rows, width), BF16),
        in_specs=[vmem] * 8,
        out_specs=vmem,
        scratch_shapes=[
            pltpu.VMEM((nf, rows, width), BF16),
            pltpu.VMEM((ns, 2, 2 * rb, inside), BF16),
            pltpu.VMEM((ns, 2, 2 * rb, 2 * quarter), BF16),
            pltpu.VMEM((4 * quarter // TILE, nf, rows, TILE), BF16),
            pltpu.VMEM((nf, WINDOW + rows, kvw), BF16),
            pltpu.VMEM((nf, 16 + rows, quarter), BF16),
            pltpu.VMEM((nf, rows, 2 * quarter), BF16),
            pltpu.VMEM((2, *aux.shape), F32),
            pltpu.VMEM((2, count // 2, rows, TILE), BF16),
            pltpu.VMEM((2, count // 2, rows, TILE), BF16),
            pltpu.VMEM((2, count, rows, TILE), BF16),
            pltpu.VMEM((2, count, rows, TILE), BF16),
            pltpu.VMEM((count, rows, TILE), F32),
            dma((2, 2)),
            dma((2, 2)),
            dma((2, 2)),
            dma((2, 2, 2, ns // 2 + 1)),
            dma((2,)),
            dma((2,)),
            dma((2,)),
            dma((2, 3)),
            dma,
            dma,
            dma((2,)),
            dma((2,)),
            dma((2,)),
            dma((2, count // 2)),
            dma((2,)),
            dma((2, count)),
        ],
        compiler_params=pltpu.CompilerParams(
            collective_id=0, has_side_effects=True, vmem_limit_bytes=62 * 1024 * 1024
        ),
        name="layer",
    )(normed, w_query, w_conv_in, w_cgate, w_bgate, kv_pack, out_pack, aux)
    return out[None]


def solution(mesh):
    placed = (
        P(("grp", "fs"), ("sp", "tp"), None),
        P(),
        P(("sp", "fs"), "tp"),
        P(("sp", "fs"), "tp"),
        P(("sp", "fs"), "tp"),
        P(None, "tp"),
        P(("sp", "fs"), "tp"),
        P(("sp", "fs"), "tp"),
        P(("sp", "fs"), "tp"),
        P("tp"),
        P("tp", ("sp", "fs")),
        P("tp", ("sp", "fs")),
    )
    return jax.shard_map(
        functools.partial(local, mesh.shape["sp"], mesh.shape["fs"]),
        mesh=mesh,
        in_specs=placed,
        out_specs=P(("grp", "fs"), ("sp", "tp"), None),
        check_vma=False,
    )
```

time: 344 us -> 187 us (0.54)
  Pallas kernels: 0 us -> 177 us
  waiting for transfers between devices: 136 us -> 0 us
  starting transfers between devices: 81.6 us -> 0 us
  matrix products: 49.1 us -> 0 us
  local copies, waits for them, and re-layouts: 37.2 us -> 4.93 us
  between operations: 13.7 us -> 0.05 us
  other arithmetic: 15 us -> 4.77 us
  blocking collectives: 9.96 us -> 0 us
    pallas_call x0 -> x1, Pallas kernels: none -> 177 us  [local(): pl.pallas_call(functools.partial(layer_kernel, ns, nf), out_shape=jax.Sha...]
    all_to_all x13 -> x0, waiting for transfers between devices: 134 us -> none  [the longest x1 95.5 us: from_everyone(): return lax.all_to_all(copies, axis, split_axis=0, concat_axis=0, tiled=True)]
    all_to_all x13 -> x0, starting transfers between devices: 75.7 us -> none  [the longest x1 30.3 us: from_everyone(): return lax.all_to_all(copies, axis, split_axis=0, concat_axis=0, tiled=True)]
    dot_general x10 -> x0, matrix products: 49.1 us -> none  [the longest x6 37.1 us: project_all(): jnp.dot(features, weight, preferred_element_type=jnp.float32)]
    all_to_all x14 -> x0, local copies, waits for them, and re-layouts: 13.7 us -> none  [the longest x6 7.65 us: local(): lax.all_to_all(shortened(rounded), 'fs', split_axis=0, concat_axis=1, til...]
    reshape x9 -> x0, local copies, waits for them, and re-layouts: 12 us -> none  [the longest x2 3.2 us: attend(): key_all[:length_here].reshape(blocks, WINDOW, kv_local, HEAD)]
    all_to_all x1 -> x0, blocking collectives: 9.96 us -> none  [summed_on_arrival(): blocks = lax.all_to_all(in_blocks(array, dim, size), axis, 0, 0, tiled=True)]
    ppermute x3 -> x0, starting transfers between devices: 5.81 us -> none  [shifted(): return lax.ppermute(array, axis, pairs)]
  transfers between devices with their start and end apart: 18 -> 0, of which waited for: 11 -> 0; matrix products, arithmetic and copies ran while one was open for 26% -> 0% of each run, Pallas kernels for 0% -> 0%
where the time goes in v1:
time: 187 us
  Pallas kernels  177 us (95%)
  local copies, waits for them, and re-layouts  4.93 us (3%)
  other arithmetic  4.77 us (3%)
    pallas_call x1, Pallas kernels, local(): pl.pallas_call(functools.partial(layer_kernel, ns, nf), out_shape=jax.Sha...  177 us

profile of v1, /device:TPU:33, one launch (start us, length us, event | category | flops | bytes accessed | tf_op | source)
XLA Modules:
  0.0 186.6 jit_solution(9686427667110565002)
XLA Ops:
  0.0 0.0 copy-start
  0.0 0.0 copy-start.1
  0.0 0.0 copy-start.2
  0.0 0.0 copy-start.4
  0.0 0.0 copy-start.3
  0.0 0.8 broadcast_in_dim.12
  0.9 1.5 fusion
  2.4 0.9 fusion.3
  3.2 0.8 fusion.4
  4.1 0.1 maximum_bitcast_fusion
  4.2 0.6 pad_maximum_fusion.2.kv_pack
  4.8 0.1 broadcast_in_dim.13
  4.8 0.0 copy-done.4
  4.9 0.6 pad_maximum_fusion.1.aux_in
  5.5 0.0 copy-done.1
  5.5 0.0 copy-done.2
  5.5 0.7 pad_maximum_fusion.out_pack
  6.2 0.0 copy-done
  6.2 0.0 copy-done.3
  6.2 1.3 fusion.2.xn
  7.4 176.9 %layer.1 = bf16[256,2048]{1,0:T(8,128)(2,1)} custom-call(bf16[256,2048]{1,0:T(8,128)(2,1)} %fusion.2.xn, bf16[32,1024]{1,0:T(8,128)(2,1)} %w_query.1, bf16[32,1024]{1,0:T(8,128)(2,1)} %w_conv_in.1, bf16[32,1024]{1,0:T(8,128)(2,1)} %w_cgate.1, bf16[32,1024]{1,0:T(8,128)(2,1)} %w_bgate.1, bf16[2,32,128]{2,1,0:T(8,128)(2,1)} %pad_maximum_fusion.2.kv_pack, ...), custom_call_target="tpu_custom_call" | custom-call | tf_op jit(solution)/shard_map/layer/pallas_call | solution.py:458
  184.3 2.3 %copy.20 = bf16[1,256,2048]{2,1,0:T(8,128)(2,1)} copy(bf16[1,256,2048]{2,1,0:T(8,128)(2,1)} %bitcast.22) | data formatting | bytes 2097152
  (3 shorter events, 0.0 us)
Async XLA Ops:
  0.0 6.2 %copy-start = (bf16[1,256,2048]{2,1,0:T(8,128)(2,1)S(1)}, bf16[1,256,2048]{2,1,0:T(8,128)(2,1)}, u32[]{:S(2)}) copy-start(bf16[1,256,2048]{2,1,0:T(8,128)(2,1)} %param.12) | copy-start | bytes 3145732
  0.0 5.5 %copy-start.1 = (bf16[1024,32]{0,1:T(8,128)(2,1)S(1)}, bf16[1024,32]{0,1:T(8,128)(2,1)}, u32[]{:S(2)}) copy-start(bf16[1024,32]{0,1:T(8,128)(2,1)} %param.23) | copy-start | bytes 196612
  0.0 5.5 %copy-start.2 = (bf16[1024,32]{0,1:T(8,128)(2,1)S(1)}, bf16[1024,32]{0,1:T(8,128)(2,1)}, u32[]{:S(2)}) copy-start(bf16[1024,32]{0,1:T(8,128)(2,1)} %param.22) | copy-start | bytes 196612
  0.0 4.8 %copy-start.4 = (bf16[3,1024]{1,0:T(4,128)(2,1)S(1)}, bf16[3,1024]{1,0:T(4,128)(2,1)}, u32[]{:S(2)}) copy-start(bf16[3,1024]{1,0:T(4,128)(2,1)} %param.17) | copy-start | bytes 18436
  0.0 6.1 %copy-start.3 = (f32[2048]{0:T(1024)S(1)}, f32[2048]{0:T(1024)}, u32[]{:S(2)}) copy-start(f32[2048]{0:T(1024)} %param.13) | copy-start | bytes 24580

commit v2 on v1

v2 whole, which is shorter than its diff:
```python
import functools

import jax
import jax.numpy as jnp
from jax import lax
from jax.experimental import pallas as pl
from jax.experimental.pallas import tpu as pltpu
from jax.sharding import PartitionSpec as P

HEAD = 64
WINDOW = 128
TAPS = 3
EPSILON = 1e-06
MESH = pl.DeviceIdType.MESH
F32 = jnp.float32
BF16 = jnp.bfloat16
TILE = 256


def rows_dot(a, b):
    return lax.dot_general(a, b, (((1,), (1,)), ((), ())), preferred_element_type=F32)


def layer_kernel(
    ns,
    nf,
    tokens,
    gain,
    w_query,
    w_conv_in,
    w_cgate,
    w_bgate,
    w_key,
    w_value,
    conv_taps,
    sinks,
    conv_out,
    attn_out,
    out,
    x_all,
    w_in,
    w_out,
    kv_pack,
    proj,
    kv_rows,
    gated,
    acts,
    aux,
    sink_rows,
    send_far,
    recv_far,
    send_near,
    recv_near,
    own_sum,
    first_send,
    first_recv,
    z_send,
    z_recv,
    y_send,
    y_recv,
    p_send,
    p_recv,
    x_send,
    x_recv,
    aux_send,
    aux_recv,
    halo_send,
    halo_recv,
    far_send,
    far_recv,
    near_send,
    near_recv,
):
    g = lax.axis_index("grp")
    s = lax.axis_index("sp")
    f = lax.axis_index("fs")
    t = lax.axis_index("tp")
    odd = lax.rem(g, 2)
    pair = g + 1 - 2 * odd
    s_next, s_prev = lax.rem(s + 1, ns), lax.rem(s + ns - 1, ns)
    f_next, f_prev = lax.rem(f + 1, nf), lax.rem(f + nf - 1, nf)
    f_far = lax.rem(f + 2, nf)
    other = 1 - t
    rows, width = tokens.shape
    rb = w_query.shape[0]
    quarter = w_query.shape[1] // 2
    kvw = w_key.shape[1]
    half = rows // 2
    blocks = rows // WINDOW

    def remote(src, dst, send_sem, recv_sem, **where):
        return pltpu.make_async_remote_copy(
            src_ref=src,
            dst_ref=dst,
            send_sem=send_sem,
            recv_sem=recv_sem,
            device_id=where,
            device_id_type=MESH,
        )

    def when(condition, body):
        if isinstance(condition, bool):
            if condition:
                body()
        else:
            pl.when(condition)(body)

    barrier = pltpu.get_barrier_semaphore()
    greeted = [
        {"fs": lax.rem(f + df, nf), "tp": lax.rem(t + dt, 2)}
        for df in range(nf)
        for dt in range(2)
        if df or dt
    ]
    greeted += [{"sp": z, "tp": lax.rem(t + dt, 2)} for z in (s_next, s_prev) for dt in range(2)]
    greeted.append({"grp": pair})
    for device in greeted:
        pl.semaphore_signal(barrier, inc=1, device_id=device, device_id_type=MESH)

    with jax.named_scope("norm"):
        step_rows = 32

        def norm(r, carry):
            span = pl.ds(pl.multiple_of(r * step_rows, step_rows), step_rows)
            wide = tokens[span, :].astype(F32)
            scale = lax.rsqrt(jnp.mean(wide * wide, axis=-1, keepdims=True) + EPSILON)
            x_all[f, span, :] = (wide * scale * gain[...]).astype(BF16)
            return carry

        lax.fori_loop(0, rows // step_rows, norm, 0)
        low = lax.broadcasted_iota(jnp.int32, (rb, kvw), 1) < HEAD
        keys_wide, values_wide = w_key[...].astype(F32), w_value[...].astype(F32)
        kv_pack[0] = jnp.where(low, keys_wide, pltpu.roll(values_wide, HEAD, 1)).astype(BF16)
        kv_pack[1] = jnp.where(low, pltpu.roll(keys_wide, HEAD, 1), values_wide).astype(BF16)
        aux[t, 0:TAPS, :] = conv_taps[...].astype(F32)
        aux[t, 8:9, 0 : sinks.shape[1]] = sinks[...]
    with jax.named_scope("meet"):
        pl.semaphore_wait(barrier, len(greeted))

    y_in, y_out = 3 * quarter // 2, quarter // 2
    z_in, z_out = y_in + quarter + kvw, 3 * quarter // 2
    weights = (w_in, w_out)
    lane = pl.multiple_of
    z_span = (pl.ds(lane(odd * y_in, 128), z_in), pl.ds(lane(odd * y_out, 128), z_out))
    y_span = (pl.ds(lane(odd * z_in, 128), y_in), pl.ds(lane(odd * z_out, 128), y_out))
    y_other = (pl.ds(lane((1 - odd) * z_in, 128), y_in), pl.ds(lane((1 - odd) * z_out, 128), y_out))
    mid = quarter // 2

    mine = f // 2
    first = lax.rem(f, 2)
    slot_rows = pl.ds(pl.multiple_of(first * rb, rb), rb)
    for k in range(2):
        for j in range(2):
            to_f = 2 * t + j
            here = jnp.logical_and(to_f == f, mine == t)
            base = j * quarter
            if k == 0:
                common = [(w_query, base, y_in, quarter), (kv_pack, None, y_in + quarter, kvw)]
                shares = (
                    [(w_conv_in, base, 0, quarter), (w_cgate, base, quarter, mid)],
                    [(w_cgate, base + mid, z_in, mid), (w_bgate, base, z_in + mid, quarter)],
                )
            else:
                common = []
                shares = (
                    [(conv_out, base, 0, quarter), (attn_out, base, quarter, mid)],
                    [(conv_out, base + mid, mid, mid), (attn_out, base, quarter, quarter)],
                )

            def deliver(moves, here=here, to_f=to_f, j=j, k=k):
                def ends(move):
                    ref, start, column, size = move
                    src = ref.at[j] if start is None else ref.at[:, pl.ds(start, size)]
                    return src, weights[k].at[s, mine, slot_rows, pl.ds(column, size)]

                @pl.when(jnp.logical_not(here))
                def _():
                    for move in moves:
                        src, dst = ends(move)
                        remote(src, dst, first_send.at[k, j], first_recv.at[k, first], fs=to_f, tp=mine).start()

                @pl.when(here)
                def _():
                    for move in moves:
                        src, dst = ends(move)
                        dst[...] = src[...]

            if common:
                deliver(common)
            for parity in range(2):
                pl.when(odd == parity)(functools.partial(deliver, shares[parity]))
        if k == 0:
            halves = (pl.ds(0, half), pl.ds(half, half))
            for which in (0, 1):
                for way, part, to in ((0, which, f_next), (1, 1 - which, f_prev)):
                    ref = x_all.at[f, halves[part]]
                    remote(ref, ref, x_send.at[way], x_recv.at[way, part], fs=to).start()
    remote(aux.at[t], aux.at[t], aux_send, aux_recv, tp=other).start()

    def wait_first(k):
        for i in range(2):
            local = jnp.logical_and(t == f // 2, f == 2 * t + i)

            @pl.when(jnp.logical_not(local))
            def _():
                piece = weights[k].at[s, t, pl.ds(i * rb, rb), z_span[k]]
                remote(piece, piece, first_send.at[k, 0], first_recv.at[k, i], tp=other).wait_recv()

    reach = ((ns // 2, ns // 2 - 1), (ns // 2 - 1, ns // 2))

    def onward(k, slot, i, way, hop):
        piece = weights[k].at[slot, t, pl.ds(i * rb, rb), z_span[k]]
        return remote(
            piece, piece, z_send.at[k, way], z_recv.at[k, way, i, hop], sp=(s_next, s_prev)[way]
        )

    def across(k, slot, i):
        piece = weights[k].at[slot, t, pl.ds(i * rb, rb), z_span[k]]
        return remote(piece, piece, p_send.at[0, k], p_recv.at[0, k], tp=other)

    def to_pair(k, slot, i, way, hop):
        piece = weights[k].at[slot, t, pl.ds(i * rb, rb), y_span[k]]
        return remote(piece, piece, y_send.at[k], y_recv.at[k, way, i, hop], grp=pair)

    def from_pair(k, slot, i, way, hop):
        piece = weights[k].at[slot, t, pl.ds(i * rb, rb), y_other[k]]
        remote(piece, piece, y_send.at[k], y_recv.at[k, way, i, hop], grp=pair).wait_recv()
        remote(piece, piece, p_send.at[1, k], p_recv.at[1, k], tp=other).start()

    def launch(k):
        for i in range(2):
            for way in range(2):
                if reach[way][i] >= 1:
                    onward(k, s, i, way, 1).start()
            to_pair(k, s, i, 0, 0).start()
        for i in range(2):
            across(k, s, i).start()

    def slot_of(way, hop):
        return lax.rem(s + ns - hop, ns) if way == 0 else lax.rem(s + hop, ns)

    def ring_step(k, hop):
        for i in range(2):
            for way in range(2):

                def body(slot=slot_of(way, hop), i=i, way=way):
                    onward(k, slot, i, way, hop).wait_recv()
                    when(hop < reach[way][i], lambda: onward(k, slot, i, way, hop + 1).start())
                    to_pair(k, slot, i, way, hop).start()
                    across(k, slot, i).start()

                when(hop <= reach[way][i], body)

    def pair_step(k, hop):
        for i in range(2):
            for way in range(2):
                body = functools.partial(from_pair, k, slot_of(way, hop), i, way, hop)
                if way == 0:
                    when(hop <= reach[way][i], body)
                elif isinstance(hop, int):
                    when(0 < hop <= reach[way][i], body)
                else:
                    when(jnp.logical_and(hop > 0, hop <= reach[way][i]), body)

    def wait_across(k):
        for n, span in ((0, z_span), (1, y_other)):
            piece = weights[k].at[:, other, :, span[k]]
            remote(piece, piece, p_send.at[n, k], p_recv.at[n, k], tp=other).wait_recv()

    last = ns // 2
    with jax.named_scope("first_wait"):
        wait_first(0)
    launch(0)
    early = max(1, ns // 4)
    with jax.named_scope("ring0_early"):
        for hop in range(1, early):
            ring_step(0, hop)
            if hop >= 2:
                pair_step(0, hop - 2)

    def x_block(which, part, way, kind):
        ref = x_all.at[which, halves[part]]
        return remote(ref, ref, x_send.at[way], x_recv.at[way, kind], fs=(f_next, f_prev)[way])

    with jax.named_scope("rows_onward"):
        x_block(f_prev, 0, 0, 0).wait_recv()
        x_block(f_prev, 0, 0, 2).start()
        x_block(f_next, 1, 1, 1).wait_recv()
        x_block(f_next, 1, 1, 2).start()
    with jax.named_scope("ring0_late"):
        for hop in range(early, last + 1):
            ring_step(0, hop)
            if hop >= 2:
                pair_step(0, hop - 2)
            if hop == max(last - 2, early):
                wait_first(1)
                launch(1)
    with jax.named_scope("pair_late"):
        for hop in range(max(last - 1, 0), last + 1):
            pair_step(0, hop)
            if hop == last - 1:
                ring_step(1, 1)
    with jax.named_scope("rows_wait"):
        x_block(f_prev, 1, 0, 1).wait_recv()
        x_block(f_next, 0, 1, 0).wait_recv()
        x_block(f_far, 0, 0, 2).wait_recv()
        x_block(f_far, 1, 1, 2).wait_recv()
    with jax.named_scope("across0"):
        wait_across(0)
    remote(aux.at[other], aux.at[other], aux_send, aux_recv, tp=other).wait_recv()

    def project(column, size):
        w = w_in[:, :, :, pl.ds(column, size)].reshape(width, size)
        a = x_all[...].reshape(nf * rows, width)
        return jnp.dot(a, w, preferred_element_type=F32).astype(BF16)

    with jax.named_scope("project_kv"):
        kv_rows[:, WINDOW:, :] = project(y_in + quarter, kvw).reshape(nf, rows, kvw)

    kv_src, kv_dst = kv_rows.at[:, pl.ds(rows, WINDOW)], kv_rows.at[:, pl.ds(0, WINDOW)]
    gated_src, gated_dst = gated.at[:, pl.ds(rows, 16)], gated.at[:, pl.ds(0, 16)]

    def send_halo(n, src, dst):
        @pl.when(t == 0)
        def _():
            remote(src, dst, halo_send.at[n], halo_recv.at[n], tp=1).start()

        @pl.when(t == 1)
        def _():
            remote(src, dst, halo_send.at[n], halo_recv.at[n], sp=s_next, tp=0).start()

    tiles = 4 * quarter // TILE

    def projection(n, carry):
        column = pl.multiple_of(n * TILE + n // 5 * kvw, 128)
        pl.when(n + 2 <= last)(lambda: ring_step(1, n + 2))
        pl.when(n <= last)(lambda: pair_step(1, n))
        proj[n] = project(column, TILE).reshape(nf, rows, TILE)
        return carry

    send_halo(0, kv_src, kv_dst)
    with jax.named_scope("projections"):
        lax.fori_loop(0, tiles, projection, 0)
        for hop in range(tiles + 2, last + 1):
            ring_step(1, hop)

    per = quarter // TILE

    def gate(q, carry):
        for n in range(per):
            product = proj[n, q].astype(F32) * proj[(2, 5)[n], q].astype(F32)
            gated[q, 16:, pl.ds(n * TILE, TILE)] = product.astype(BF16)
        return carry

    with jax.named_scope("gates"):
        lax.fori_loop(0, nf, gate, 0)
        aux_lane = lax.broadcasted_iota(jnp.int32, (1, 128), 1)
        heads = quarter // HEAD
        held = aux[f // 2, 8:9, 0:128]
        for h in range(heads):
            one = jnp.sum(jnp.where(aux_lane == first * heads + h, held, 0.0), axis=-1, keepdims=True)
            sink_rows[h : h + 1, :] = jnp.broadcast_to(one * HEAD**0.5, (1, 128))
    send_halo(1, gated_src, gated_dst)

    at_start = jnp.logical_and(s == 0, t == 0)

    key_id = lax.broadcasted_iota(jnp.int32, (2 * WINDOW, WINDOW), 0)
    query_id = lax.broadcasted_iota(jnp.int32, (2 * WINDOW, WINDOW), 1)
    low_keys = lax.broadcasted_iota(jnp.int32, (2 * WINDOW, kvw), 1) < HEAD

    def attend(step, carry):
        q = step // blocks
        b = lax.rem(step, blocks)
        begin = pl.multiple_of(b * WINDOW, WINDOW)
        both = kv_rows[q, pl.ds(begin, 2 * WINDOW), :].astype(F32)
        turned = pltpu.roll(both, HEAD, 1)
        zero = jnp.zeros_like(both)
        keys = jnp.concatenate([jnp.where(low_keys, both, zero), jnp.where(low_keys, zero, turned)], 0).astype(BF16)
        values = jnp.concatenate([jnp.where(low_keys, turned, zero), jnp.where(low_keys, zero, both)], 0)
        values = jnp.transpose(values).astype(BF16)
        first_key = jnp.where(jnp.logical_and(at_start, b == 0), WINDOW, 0)
        allowed = (key_id > query_id) & (key_id <= query_id + WINDOW) & (key_id >= first_key)
        for duo in range(quarter // (2 * HEAD)):
            n, column = 3 + duo * 2 * HEAD // TILE, duo * 2 * HEAD % TILE
            queries = proj[n, q, pl.ds(begin, WINDOW), column : column + 2 * HEAD]
            scores = rows_dot(keys, queries)
            probs = []
            for h in range(2):
                score = jnp.where(allowed, scores[h * 2 * WINDOW : (h + 1) * 2 * WINDOW], -jnp.inf)
                sink = sink_rows[2 * duo + h : 2 * duo + h + 1, :]
                peak = jnp.maximum(jnp.max(score, axis=0, keepdims=True), sink)
                weight = jnp.exp((score - peak) * (1.0 / HEAD**0.5))
                total = jnp.sum(weight, axis=0, keepdims=True) + jnp.exp((sink - peak) * (1.0 / HEAD**0.5))
                probs.append((weight * (1.0 / total)).astype(BF16))
            attended = jnp.dot(values, jnp.concatenate(probs, 0), preferred_element_type=F32)
            span = pl.ds(quarter + duo * 2 * HEAD, 2 * HEAD)
            acts[q, pl.ds(begin, WINDOW), span] = jnp.transpose(attended).astype(BF16)
        return carry

    with jax.named_scope("halo_wait"):
        remote(kv_dst, kv_dst, halo_send.at[0], halo_recv.at[0], tp=other).wait_recv()
    with jax.named_scope("attention"):
        lax.fori_loop(0, nf * blocks, attend, 0)

    remote(gated_dst, gated_dst, halo_send.at[1], halo_recv.at[1], tp=other).wait_recv()

    @pl.when(at_start)
    def _():
        gated[:, 0:16, :] = jnp.zeros_like(gated[:, 0:16, :])

    def convolve(q, carry):
        for n in range(per):
            span = pl.ds(n * TILE, TILE)
            wide = gated[q, :, span].astype(F32)
            taps = aux[f // 2, 0:TAPS, pl.ds(pl.multiple_of(first * quarter + n * TILE, TILE), TILE)]
            total = (
                pltpu.roll(wide, 2, 0)[16:] * taps[0:1]
                + pltpu.roll(wide, 1, 0)[16:] * taps[1:2]
                + wide[16:] * taps[2:3]
            )
            acts[q, :, span] = (proj[6 + n, q].astype(F32) * total).astype(BF16)
        return carry

    with jax.named_scope("convolution"):
        lax.fori_loop(0, nf, convolve, 0)

    with jax.named_scope("across1"):
        for hop in range(tiles, last + 1):
            pair_step(1, hop)
        wait_across(1)
    count = width // TILE
    near_half = count // 2
    chips = TILE // (2 * 2 * rb)

    def partial(q, n):
        w = w_out[pl.ds(n * chips, chips)].reshape(TILE, 2 * quarter)
        return rows_dot(acts[q], w)

    ways = (f_next, f_prev)

    def far_copy(way, n):
        return remote(send_far.at[way, n], recv_far.at[way, n], far_send.at[way], far_recv.at[way, n], fs=ways[way])

    def near_copy(way, n):
        return remote(
            send_near.at[way, n], recv_near.at[way, n], near_send.at[way], near_recv.at[way, n], fs=ways[way]
        )

    def far_step(n, carry):
        send_far[0, n] = partial(f_far, n).astype(BF16)
        send_far[1, n] = partial(f_far, n + near_half).astype(BF16)
        far_copy(0, n).start()
        far_copy(1, n).start()
        return carry

    def plain_step(n, carry):
        send_near[0, n + near_half] = partial(f_next, n + near_half).astype(BF16)
        send_near[1, n] = partial(f_prev, n).astype(BF16)
        near_copy(0, n + near_half).start()
        near_copy(1, n).start()
        return carry

    def joined_step(n, carry):
        right, left = partial(f_next, n), partial(f_prev, n + near_half)
        far_copy(0, n).wait_recv()
        far_copy(1, n).wait_recv()
        send_near[0, n] = (right + recv_far[0, n].astype(F32)).astype(BF16)
        send_near[1, n + near_half] = (left + recv_far[1, n].astype(F32)).astype(BF16)
        near_copy(0, n).start()
        near_copy(1, n + near_half).start()
        return carry

    def own_step(n, carry):
        own_sum[n] = partial(f, n)
        return carry

    with jax.named_scope("far"):
        lax.fori_loop(0, near_half, far_step, 0)
    with jax.named_scope("plain"):
        lax.fori_loop(0, near_half, plain_step, 0)
    with jax.named_scope("joined"):
        lax.fori_loop(0, near_half, joined_step, 0)
    with jax.named_scope("own"):
        lax.fori_loop(0, count, own_step, 0)
    with jax.named_scope("finish"):
        for n in range(near_half):
            for way, tile in ((0, n + near_half), (1, n)):
                near_copy(way, tile).wait_recv()
        for n in range(near_half):
            for way, tile in ((0, n), (1, n + near_half)):
                near_copy(way, tile).wait_recv()
            for tile in (n, n + near_half):
                total = own_sum[tile] + recv_near[0, tile].astype(F32) + recv_near[1, tile].astype(F32)
                out[:, tile * TILE : (tile + 1) * TILE] = total.astype(BF16)

    for k in range(2):
        for j in range(2):
            here = jnp.logical_and(2 * t + j == f, mine == t)

            @pl.when(jnp.logical_not(here))
            def _():
                piece = weights[k].at[s, t, pl.ds(0, rb), z_span[k]]
                remote(piece, piece, first_send.at[k, j], first_recv.at[k, 0], tp=other).wait_send()

        for way in range(2):
            pieces = weights[k].at[pl.ds(0, ns - 1), 0, pl.ds(0, rb), z_span[k]]
            remote(pieces, pieces, z_send.at[k, way], z_recv.at[k, way, 0, 0], tp=other).wait_send()
        for n, span in ((0, z_span), (1, y_other)):
            piece = weights[k].at[:, t, :, span[k]]
            remote(piece, piece, p_send.at[n, k], p_recv.at[n, k], tp=other).wait_send()
        piece = weights[k].at[:, t, :, y_span[k]]
        remote(piece, piece, y_send.at[k], y_recv.at[k, 0, 0, 0], tp=other).wait_send()
    for way in range(2):
        ref = x_all.at[pl.ds(0, 3), halves[0]]
        remote(ref, ref, x_send.at[way], x_recv.at[way, 0], tp=other).wait_send()
        remote(send_far.at[way], send_far.at[way], far_send.at[way], far_recv.at[way, 0], tp=other).wait_send()
        remote(send_near.at[way], send_near.at[way], near_send.at[way], near_recv.at[way, 0], tp=other).wait_send()
    remote(aux.at[t], aux.at[t], aux_send, aux_recv, tp=other).wait_send()
    remote(kv_src, kv_src, halo_send.at[0], halo_recv.at[0], tp=other).wait_send()
    remote(gated_src, gated_src, halo_send.at[1], halo_recv.at[1], tp=other).wait_send()


def local(
    ns,
    nf,
    tokens,
    norm_gain,
    w_bgate,
    w_cgate,
    w_conv_in,
    conv_taps,
    w_query,
    w_key,
    w_value,
    sink_logits,
    conv_out_weight,
    attn_out_weight,
):
    rows, width = tokens.shape[1:]
    rb, columns = w_query.shape
    quarter = columns // 2
    kvw = w_key.shape[1]
    count = width // TILE
    inside = 4 * quarter + kvw
    vmem = pl.BlockSpec(memory_space=pltpu.VMEM)
    dma = pltpu.SemaphoreType.DMA
    out = pl.pallas_call(
        functools.partial(layer_kernel, ns, nf),
        out_shape=jax.ShapeDtypeStruct((rows, width), BF16),
        in_specs=[vmem] * 12,
        out_specs=vmem,
        scratch_shapes=[
            pltpu.VMEM((nf, rows, width), BF16),
            pltpu.VMEM((ns, 2, 2 * rb, inside), BF16),
            pltpu.VMEM((ns, 2, 2 * rb, 2 * quarter), BF16),
            pltpu.VMEM((2, rb, kvw), BF16),
            pltpu.VMEM((4 * quarter // TILE, nf, rows, TILE), BF16),
            pltpu.VMEM((nf, WINDOW + rows, kvw), BF16),
            pltpu.VMEM((nf, 16 + rows, quarter), BF16),
            pltpu.VMEM((nf, rows, 2 * quarter), BF16),
            pltpu.VMEM((2, 16, columns), F32),
            pltpu.VMEM((quarter // HEAD, 128), F32),
            pltpu.VMEM((2, count // 2, rows, TILE), BF16),
            pltpu.VMEM((2, count // 2, rows, TILE), BF16),
            pltpu.VMEM((2, count, rows, TILE), BF16),
            pltpu.VMEM((2, count, rows, TILE), BF16),
            pltpu.VMEM((count, rows, TILE), F32),
            dma((2, 2)),
            dma((2, 2)),
            dma((2, 2)),
            dma((2, 2, 2, ns // 2 + 1)),
            dma((2,)),
            dma((2, 2, 2, ns // 2 + 1)),
            dma((2, 2)),
            dma((2, 2)),
            dma((2,)),
            dma((2, 3)),
            dma,
            dma,
            dma((2,)),
            dma((2,)),
            dma((2,)),
            dma((2, count // 2)),
            dma((2,)),
            dma((2, count)),
        ],
        compiler_params=pltpu.CompilerParams(
            collective_id=0, has_side_effects=True, vmem_limit_bytes=62 * 1024 * 1024
        ),
        name="layer",
    )(
        tokens[0],
        norm_gain[None],
        w_query,
        w_conv_in,
        w_cgate,
        w_bgate,
        w_key,
        w_value,
        conv_taps,
        sink_logits[None],
        conv_out_weight.T,
        attn_out_weight.T,
    )
    return out[None]


def solution(mesh):
    placed = (
        P(("grp", "fs"), ("sp", "tp"), None),
        P(),
        P(("sp", "fs"), "tp"),
        P(("sp", "fs"), "tp"),
        P(("sp", "fs"), "tp"),
        P(None, "tp"),
        P(("sp", "fs"), "tp"),
        P(("sp", "fs"), "tp"),
        P(("sp", "fs"), "tp"),
        P("tp"),
        P("tp", ("sp", "fs")),
        P("tp", ("sp", "fs")),
    )
    return jax.shard_map(
        functools.partial(local, mesh.shape["sp"], mesh.shape["fs"]),
        mesh=mesh,
        in_specs=placed,
        out_specs=P(("grp", "fs"), ("sp", "tp"), None),
        check_vma=False,
    )
```

time: 187 us -> 150 us (0.80)
  Pallas kernels: 177 us -> 148 us
  other arithmetic: 4.77 us -> 0 us
  local copies, waits for them, and re-layouts: 4.93 us -> 2.3 us
    pallas_call x1, Pallas kernels: 177 us -> 148 us  [local(): pl.pallas_call(functools.partial(layer_kernel, ns, nf), out_shape=jax.Sha...]
where the time goes in v2:
time: 150 us
  Pallas kernels  148 us (99%)
  local copies, waits for them, and re-layouts  2.3 us (2%)
    pallas_call x1, Pallas kernels, local(): pl.pallas_call(functools.partial(layer_kernel, ns, nf), out_shape=jax.Sha...  148 us

profile of v2, /device:TPU:33, one launch (start us, length us, event | category | flops | bytes accessed | tf_op | source)
XLA Modules:
  0.0 149.9 jit_solution(7071994033241489843)
XLA Ops:
  0.0 147.6 %layer.1 = bf16[256,2048]{1,0:T(8,128)(2,1)} custom-call(bf16[256,2048]{1,0:T(8,128)(2,1)} %bitcast.7, f32[1,2048]{1,0:T(1,128)} %bitcast.10, bf16[32,1024]{1,0:T(8,128)(2,1)} %w_query.1, bf16[32,1024]{1,0:T(8,128)(2,1)} %w_conv_in.1, bf16[32,1024]{1,0:T(8,128)(2,1)} %w_cgate.1, bf16[32,1024]{1,0:T(8,128)(2,1)} %w_bgate.1, bf16[32,128]{1,0:T(8,128)(2,1)} %w_key.1, ...), custom_call_target="tpu_custom_call" | custom-call | tf_op jit(solution)/shard_map/layer/pallas_call | solution.py:547
  147.6 2.3 %copy.14 = bf16[1,256,2048]{2,1,0:T(8,128)(2,1)} copy(bf16[1,256,2048]{2,1,0:T(8,128)(2,1)} %bitcast.6) | data formatting | bytes 2097152

commit v3 on v2

--- a/solution.py
+++ b/solution.py
@@ -24,53 +24,46 @@
 def layer_kernel(
     ns,
     nf,
-    tokens,
-    gain,
-    w_query,
-    w_conv_in,
-    w_cgate,
-    w_bgate,
-    w_key,
-    w_value,
-    conv_taps,
-    sinks,
-    conv_out,
-    attn_out,
-    out,
-    x_all,
-    w_in,
-    w_out,
-    kv_pack,
-    proj,
-    kv_rows,
-    gated,
-    acts,
-    aux,
-    sink_rows,
-    send_far,
-    recv_far,
-    send_near,
-    recv_near,
-    own_sum,
-    first_send,
-    first_recv,
-    z_send,
-    z_recv,
-    y_send,
-    y_recv,
-    p_send,
-    p_recv,
-    x_send,
-    x_recv,
-    aux_send,
-    aux_recv,
-    halo_send,
-    halo_recv,
-    far_send,
-    far_recv,
-    near_send,
-    near_recv,
+    *refs,
 ):
+    given, out, held, rest = refs[:12], refs[12], refs[13:25], refs[25:]
+    tokens, gain, w_query, w_conv_in, w_cgate, w_bgate, w_key, w_value, conv_taps, sinks, conv_out, attn_out = held
+    (
+        x_all,
+        w_in,
+        w_out,
+        kv_pack,
+        proj,
+        kv_rows,
+        gated,
+        acts,
+        aux,
+        sink_rows,
+        send_far,
+        recv_far,
+        send_near,
+        recv_near,
+        own_sum,
+        first_send,
+        first_recv,
+        z_send,
+        z_recv,
+        y_send,
+        y_recv,
+        p_send,
+        p_recv,
+        x_send,
+        x_recv,
+        aux_send,
+        aux_recv,
+        halo_send,
+        halo_recv,
+        far_send,
+        far_recv,
+        near_send,
+        near_recv,
+        load_sem,
+    ) = rest
     g = lax.axis_index("grp")
     s = lax.axis_index("sp")
     f = lax.axis_index("fs")
@@ -81,6 +74,11 @@
     f_next, f_prev = lax.rem(f + 1, nf), lax.rem(f + nf - 1, nf)
     f_far = lax.rem(f + 2, nf)
     other = 1 - t
+
+    def seat(q):
+        return lax.rem(q, 2) * 2 + q // 2
+
+    mine_seat, far_seat, next_seat, prev_seat = seat(f), seat(f_far), seat(f_next), seat(f_prev)
     rows, width = tokens.shape
     rb = w_query.shape[0]
     quarter = w_query.shape[1] // 2
@@ -97,6 +95,10 @@
             device_id=where,
             device_id_type=MESH,
         )
+
+    loads = [pltpu.make_async_copy(a, b, load_sem.at[n]) for n, (a, b) in enumerate(zip(given, held))]
+    for n in (*range(1, len(loads)), 0):
+        loads[n].start()
 
     def when(condition, body):
         if isinstance(condition, bool):
@@ -117,17 +119,9 @@
     for device in greeted:
         pl.semaphore_signal(barrier, inc=1, device_id=device, device_id_type=MESH)
 
-    with jax.named_scope("norm"):
-        step_rows = 32
-
-        def norm(r, carry):
-            span = pl.ds(pl.multiple_of(r * step_rows, step_rows), step_rows)
-            wide = tokens[span, :].astype(F32)
-            scale = lax.rsqrt(jnp.mean(wide * wide, axis=-1, keepdims=True) + EPSILON)
-            x_all[f, span, :] = (wide * scale * gain[...]).astype(BF16)
-            return carry
-
-        lax.fori_loop(0, rows // step_rows, norm, 0)
+    with jax.named_scope("pack"):
+        for load in loads[1:]:
+            load.wait()
         low = lax.broadcasted_iota(jnp.int32, (rb, kvw), 1) < HEAD
         keys_wide, values_wide = w_key[...].astype(F32), w_value[...].astype(F32)
         kv_pack[0] = jnp.where(low, keys_wide, pltpu.roll(values_wide, HEAD, 1)).astype(BF16)
@@ -149,7 +143,7 @@
     mine = f // 2
     first = lax.rem(f, 2)
     slot_rows = pl.ds(pl.multiple_of(first * rb, rb), rb)
-    for k in range(2):
+    def first_exchange(k):
         for j in range(2):
             to_f = 2 * t + j
             here = jnp.logical_and(to_f == f, mine == t)
@@ -189,12 +183,20 @@
                 deliver(common)
             for parity in range(2):
                 pl.when(odd == parity)(functools.partial(deliver, shares[parity]))
-        if k == 0:
-            halves = (pl.ds(0, half), pl.ds(half, half))
-            for which in (0, 1):
-                for way, part, to in ((0, which, f_next), (1, 1 - which, f_prev)):
-                    ref = x_all.at[f, halves[part]]
-                    remote(ref, ref, x_send.at[way], x_recv.at[way, part], fs=to).start()
+
+    first_exchange(0)
+    with jax.named_scope("norm"):
+        loads[0].wait()
+        step_rows = 32
+
+        def norm(r, carry):
+            span = pl.ds(pl.multiple_of(r * step_rows, step_rows), step_rows)
+            wide = tokens[span, :].astype(F32)
+            scale = lax.rsqrt(jnp.mean(wide * wide, axis=-1, keepdims=True) + EPSILON)
+            x_all[mine_seat, span, :] = (wide * scale * gain[...]).astype(BF16)
+            return carry
+
+        lax.fori_loop(0, rows // step_rows, norm, 0)
     remote(aux.at[t], aux.at[t], aux_send, aux_recv, tp=other).start()
 
     def wait_first(k):
@@ -239,39 +241,64 @@
     def slot_of(way, hop):
         return lax.rem(s + ns - hop, ns) if way == 0 else lax.rem(s + hop, ns)
 
+    def ring_part(k, hop, i):
+        for way in range(2):
+
+            def body(slot=slot_of(way, hop), way=way):
+                onward(k, slot, i, way, hop).wait_recv()
+                when(hop < reach[way][i], lambda: onward(k, slot, i, way, hop + 1).start())
+                to_pair(k, slot, i, way, hop).start()
+                across(k, slot, i).start()
+
+            when(hop <= reach[way][i], body)
+
+    def pair_part(k, hop, i):
+        for way in range(2):
+            body = functools.partial(from_pair, k, slot_of(way, hop), i, way, hop)
+            if isinstance(hop, int):
+                when(way <= hop <= reach[way][i], body)
+            else:
+                when(jnp.logical_and(hop >= way, hop <= reach[way][i]), body)
+
     def ring_step(k, hop):
         for i in range(2):
-            for way in range(2):
-
-                def body(slot=slot_of(way, hop), i=i, way=way):
-                    onward(k, slot, i, way, hop).wait_recv()
-                    when(hop < reach[way][i], lambda: onward(k, slot, i, way, hop + 1).start())
-                    to_pair(k, slot, i, way, hop).start()
-                    across(k, slot, i).start()
-
-                when(hop <= reach[way][i], body)
+            ring_part(k, hop, i)
 
     def pair_step(k, hop):
         for i in range(2):
-            for way in range(2):
-                body = functools.partial(from_pair, k, slot_of(way, hop), i, way, hop)
-                if way == 0:
-                    when(hop <= reach[way][i], body)
-                elif isinstance(hop, int):
-                    when(0 < hop <= reach[way][i], body)
-                else:
-                    when(jnp.logical_and(hop > 0, hop <= reach[way][i]), body)
+            pair_part(k, hop, i)
+
+    lag = 2
+
+    def ring_half(k, u):
+        hop = u // 2
+        for i in range(2):
+
+            @pl.when(lax.rem(u, 2) == i)
+            def _():
+                pl.when(jnp.logical_and(hop >= 1, hop <= last))(lambda: ring_part(k, hop, i))
+                pl.when(jnp.logical_and(hop >= lag, hop <= last + lag))(lambda: pair_part(k, hop - lag, i))
+
+    last = ns // 2
 
     def wait_across(k):
         for n, span in ((0, z_span), (1, y_other)):
             piece = weights[k].at[:, other, :, span[k]]
             remote(piece, piece, p_send.at[n, k], p_recv.at[n, k], tp=other).wait_recv()
 
-    last = ns // 2
     with jax.named_scope("first_wait"):
         wait_first(0)
     launch(0)
+    halves = (pl.ds(0, half), pl.ds(half, half))
+    for which in (0, 1):
+        for way, part, to in ((0, which, f_next), (1, 1 - which, f_prev)):
+            ref = x_all.at[mine_seat, halves[part]]
+            remote(ref, ref, x_send.at[way], x_recv.at[way, part], fs=to).start()
+    first_exchange(1)
     early = max(1, ns // 4)
+    start_out = max(last - 2, early)
+    ahead = min(1, start_out - 1)
+    resume = 2 * (last - start_out + ahead + 1)
     with jax.named_scope("ring0_early"):
         for hop in range(1, early):
             ring_step(0, hop)
@@ -283,42 +310,47 @@
         return remote(ref, ref, x_send.at[way], x_recv.at[way, kind], fs=(f_next, f_prev)[way])
 
     with jax.named_scope("rows_onward"):
-        x_block(f_prev, 0, 0, 0).wait_recv()
-        x_block(f_prev, 0, 0, 2).start()
-        x_block(f_next, 1, 1, 1).wait_recv()
-        x_block(f_next, 1, 1, 2).start()
+        x_block(prev_seat, 0, 0, 0).wait_recv()
+        x_block(prev_seat, 0, 0, 2).start()
+        x_block(next_seat, 1, 1, 1).wait_recv()
+        x_block(next_seat, 1, 1, 2).start()
     with jax.named_scope("ring0_late"):
         for hop in range(early, last + 1):
             ring_step(0, hop)
             if hop >= 2:
                 pair_step(0, hop - 2)
-            if hop == max(last - 2, early):
+            if hop == start_out:
                 wait_first(1)
                 launch(1)
+            if hop > start_out:
+                ring_step(1, hop - start_out)
     with jax.named_scope("pair_late"):
         for hop in range(max(last - 1, 0), last + 1):
             pair_step(0, hop)
-            if hop == last - 1:
-                ring_step(1, 1)
+            if 1 <= hop + ahead - last <= ahead:
+                ring_step(1, last - start_out + hop + ahead - last)
+        for hop in range(0, max(resume // 2 - lag, 0)):
+            pair_step(1, hop)
     with jax.named_scope("rows_wait"):
-        x_block(f_prev, 1, 0, 1).wait_recv()
-        x_block(f_next, 0, 1, 0).wait_recv()
-        x_block(f_far, 0, 0, 2).wait_recv()
-        x_block(f_far, 1, 1, 2).wait_recv()
+        x_block(prev_seat, 1, 0, 1).wait_recv()
+        x_block(next_seat, 0, 1, 0).wait_recv()
+        x_block(far_seat, 0, 0, 2).wait_recv()
+        x_block(far_seat, 1, 1, 2).wait_recv()
     with jax.named_scope("across0"):
         wait_across(0)
     remote(aux.at[other], aux.at[other], aux_send, aux_recv, tp=other).wait_recv()
 
-    def project(column, size):
+    def project(base, column, size):
         w = w_in[:, :, :, pl.ds(column, size)].reshape(width, size)
-        a = x_all[...].reshape(nf * rows, width)
+        a = x_all[pl.ds(base, 2)].reshape(2 * rows, width)
         return jnp.dot(a, w, preferred_element_type=F32).astype(BF16)
 
-    with jax.named_scope("project_kv"):
-        kv_rows[:, WINDOW:, :] = project(y_in + quarter, kvw).reshape(nf, rows, kvw)
-
-    kv_src, kv_dst = kv_rows.at[:, pl.ds(rows, WINDOW)], kv_rows.at[:, pl.ds(0, WINDOW)]
-    gated_src, gated_dst = gated.at[:, pl.ds(rows, 16)], gated.at[:, pl.ds(0, 16)]
+    def halo_refs(ref, base, tail):
+        here = ref.at[pl.ds(base, 2)]
+        return here.at[:, pl.ds(rows, tail)], here.at[:, pl.ds(0, tail)]
+
+    def halo_copies(base, turn):
+        return ((turn, *halo_refs(kv_rows, base, WINDOW)), (2 + turn, *halo_refs(gated, base, 16)))
 
     def send_halo(n, src, dst):
         @pl.when(t == 0)
@@ -329,20 +361,10 @@
         def _():
             remote(src, dst, halo_send.at[n], halo_recv.at[n], sp=s_next, tp=0).start()
 
+    def wait_halo(n, src, dst):
+        remote(dst, dst, halo_send.at[n], halo_recv.at[n], tp=other).wait_recv()
+
     tiles = 4 * quarter // TILE
-
-    def projection(n, carry):
-        column = pl.multiple_of(n * TILE + n // 5 * kvw, 128)
-        pl.when(n + 2 <= last)(lambda: ring_step(1, n + 2))
-        pl.when(n <= last)(lambda: pair_step(1, n))
-        proj[n] = project(column, TILE).reshape(nf, rows, TILE)
-        return carry
-
-    send_halo(0, kv_src, kv_dst)
-    with jax.named_scope("projections"):
-        lax.fori_loop(0, tiles, projection, 0)
-        for hop in range(tiles + 2, last + 1):
-            ring_step(1, hop)
 
     per = quarter // TILE
 
@@ -352,61 +374,54 @@
             gated[q, 16:, pl.ds(n * TILE, TILE)] = product.astype(BF16)
         return carry
 
-    with jax.named_scope("gates"):
-        lax.fori_loop(0, nf, gate, 0)
+    with jax.named_scope("sinks"):
         aux_lane = lax.broadcasted_iota(jnp.int32, (1, 128), 1)
         heads = quarter // HEAD
         held = aux[f // 2, 8:9, 0:128]
         for h in range(heads):
             one = jnp.sum(jnp.where(aux_lane == first * heads + h, held, 0.0), axis=-1, keepdims=True)
             sink_rows[h : h + 1, :] = jnp.broadcast_to(one * HEAD**0.5, (1, 128))
-    send_halo(1, gated_src, gated_dst)
 
     at_start = jnp.logical_and(s == 0, t == 0)
 
-    key_id = lax.broadcasted_iota(jnp.int32, (2 * WINDOW, WINDOW), 0)
-    query_id = lax.broadcasted_iota(jnp.int32, (2 * WINDOW, WINDOW), 1)
+    key_id = lax.broadcasted_iota(jnp.int32, (WINDOW, WINDOW), 0)
+    query_id = lax.broadcasted_iota(jnp.int32, (WINDOW, WINDOW), 1)
+    before = key_id > query_id
     low_keys = lax.broadcasted_iota(jnp.int32, (2 * WINDOW, kvw), 1) < HEAD
-
-    def attend(step, carry):
-        q = step // blocks
-        b = lax.rem(step, blocks)
-        begin = pl.multiple_of(b * WINDOW, WINDOW)
-        both = kv_rows[q, pl.ds(begin, 2 * WINDOW), :].astype(F32)
+    duos = quarter // (2 * HEAD)
+    scale = 1.0 / HEAD**0.5
+
+    def attend_block(q, b):
+        begin = b * WINDOW
+        both = kv_rows[q, begin : begin + 2 * WINDOW, :].astype(F32)
         turned = pltpu.roll(both, HEAD, 1)
         zero = jnp.zeros_like(both)
         keys = jnp.concatenate([jnp.where(low_keys, both, zero), jnp.where(low_keys, zero, turned)], 0).astype(BF16)
         values = jnp.concatenate([jnp.where(low_keys, turned, zero), jnp.where(low_keys, zero, both)], 0)
         values = jnp.transpose(values).astype(BF16)
-        first_key = jnp.where(jnp.logical_and(at_start, b == 0), WINDOW, 0)
-        allowed = (key_id > query_id) & (key_id <= query_id + WINDOW) & (key_id >= first_key)
-        for duo in range(quarter // (2 * HEAD)):
+        scores = []
+        for duo in range(duos):
             n, column = 3 + duo * 2 * HEAD // TILE, duo * 2 * HEAD % TILE
-            queries = proj[n, q, pl.ds(begin, WINDOW), column : column + 2 * HEAD]
-            scores = rows_dot(keys, queries)
-            probs = []
+            scores.append(rows_dot(keys, proj[n, q, begin : begin + WINDOW, column : column + 2 * HEAD]))
+        probs = []
+        for duo in range(duos):
+            parts = []
             for h in range(2):
-                score = jnp.where(allowed, scores[h * 2 * WINDOW : (h + 1) * 2 * WINDOW], -jnp.inf)
+                old = scores[duo][2 * h * WINDOW : (2 * h + 1) * WINDOW]
+                if b == 0:
+                    old = jnp.where(at_start, -jnp.inf, old)
+                score = jnp.where(before, old, scores[duo][(2 * h + 1) * WINDOW : (2 * h + 2) * WINDOW])
                 sink = sink_rows[2 * duo + h : 2 * duo + h + 1, :]
                 peak = jnp.maximum(jnp.max(score, axis=0, keepdims=True), sink)
-                weight = jnp.exp((score - peak) * (1.0 / HEAD**0.5))
-                total = jnp.sum(weight, axis=0, keepdims=True) + jnp.exp((sink - peak) * (1.0 / HEAD**0.5))
-                probs.append((weight * (1.0 / total)).astype(BF16))
-            attended = jnp.dot(values, jnp.concatenate(probs, 0), preferred_element_type=F32)
+                weight = jnp.exp((score - peak) * scale)
+                total = jnp.sum(weight, axis=0, keepdims=True) + jnp.exp((sink - peak) * scale)
+                prob = weight * (1.0 / total)
+                parts += [jnp.where(before, prob, 0.0).astype(BF16), jnp.where(before, 0.0, prob).astype(BF16)]
+            probs.append(jnp.concatenate(parts, 0))
+        for duo in range(duos):
+            attended = jnp.dot(values, probs[duo], preferred_element_type=F32)
             span = pl.ds(quarter + duo * 2 * HEAD, 2 * HEAD)
-            acts[q, pl.ds(begin, WINDOW), span] = jnp.transpose(attended).astype(BF16)
-        return carry
-
-    with jax.named_scope("halo_wait"):
-        remote(kv_dst, kv_dst, halo_send.at[0], halo_recv.at[0], tp=other).wait_recv()
-    with jax.named_scope("attention"):
-        lax.fori_loop(0, nf * blocks, attend, 0)
-
-    remote(gated_dst, gated_dst, halo_send.at[1], halo_recv.at[1], tp=other).wait_recv()
-
-    @pl.when(at_start)
-    def _():
-        gated[:, 0:16, :] = jnp.zeros_like(gated[:, 0:16, :])
+            acts[q, begin : begin + WINDOW, span] = jnp.transpose(attended).astype(BF16)
 
     def convolve(q, carry):
         for n in range(per):
@@ -421,13 +436,6 @@
             acts[q, :, span] = (proj[6 + n, q].astype(F32) * total).astype(BF16)
         return carry
 
-    with jax.named_scope("convolution"):
-        lax.fori_loop(0, nf, convolve, 0)
-
-    with jax.named_scope("across1"):
-        for hop in range(tiles, last + 1):
-            pair_step(1, hop)
-        wait_across(1)
     count = width // TILE
     near_half = count // 2
     chips = TILE // (2 * 2 * rb)
@@ -447,21 +455,21 @@
         )
 
     def far_step(n, carry):
-        send_far[0, n] = partial(f_far, n).astype(BF16)
-        send_far[1, n] = partial(f_far, n + near_half).astype(BF16)
+        send_far[0, n] = partial(far_seat, n).astype(BF16)
+        send_far[1, n] = partial(far_seat, n + near_half).astype(BF16)
         far_copy(0, n).start()
         far_copy(1, n).start()
         return carry
 
     def plain_step(n, carry):
-        send_near[0, n + near_half] = partial(f_next, n + near_half).astype(BF16)
-        send_near[1, n] = partial(f_prev, n).astype(BF16)
+        send_near[0, n + near_half] = partial(next_seat, n + near_half).astype(BF16)
+        send_near[1, n] = partial(prev_seat, n).astype(BF16)
         near_copy(0, n + near_half).start()
         near_copy(1, n).start()
         return carry
 
     def joined_step(n, carry):
-        right, left = partial(f_next, n), partial(f_prev, n + near_half)
+        right, left = partial(next_seat, n), partial(prev_seat, n + near_half)
         far_copy(0, n).wait_recv()
         far_copy(1, n).wait_recv()
         send_near[0, n] = (right + recv_far[0, n].astype(F32)).astype(BF16)
@@ -471,13 +479,62 @@
         return carry
 
     def own_step(n, carry):
-        own_sum[n] = partial(f, n)
+        own_sum[n] = partial(mine_seat, n)
         return carry
 
+    def sequences(turn, carry):
+        base = lax.rem(f + 1 + turn, 2) * 2
+        kv_halo, gated_halo = halo_copies(base, turn)
+        count_from = resume + turn * 4 * (last + lag)
+
+        def projection(n, inner):
+            ring_half(1, count_from + n)
+            pl.when(n == 1)(lambda: send_halo(*kv_halo))
+            column = pl.multiple_of(n * TILE + n // 5 * kvw, 128)
+            proj[n, pl.ds(base, 2)] = project(base, column, TILE).reshape(2, rows, TILE)
+            return inner
+
+        def attend(r, inner):
+            for b in range(blocks):
+                ring_half(1, count_from + tiles + r * blocks + b)
+                attend_block(base + r, b)
+                if b == 0:
+                    pl.when(r == 0)(lambda: send_halo(*gated_halo))
+            return inner
+
+        with jax.named_scope("project_kv"):
+            kv_rows[pl.ds(base, 2), WINDOW:, :] = project(base, y_in + quarter, kvw).reshape(2, rows, kvw)
+        with jax.named_scope("projections"):
+            lax.fori_loop(0, tiles, projection, 0)
+        with jax.named_scope("gates"):
+            lax.fori_loop(base, base + 2, gate, 0)
+        with jax.named_scope("halo_wait"):
+            wait_halo(*kv_halo)
+        with jax.named_scope("attention"):
+            lax.fori_loop(0, 2, attend, 0)
+        with jax.named_scope("gated_wait"):
+            wait_halo(*gated_halo)
+
+        @pl.when(at_start)
+        def _():
+            gated[pl.ds(base, 2), 0:16, :] = jnp.zeros((2, 16, quarter), BF16)
+
+        with jax.named_scope("convolution"):
+            lax.fori_loop(base, base + 2, convolve, 0)
+
+        @pl.when(turn == 0)
+        def _():
+            with jax.named_scope("across1"):
+                lax.fori_loop(resume + tiles + 2 * blocks, 2 * (last + lag) + 2, lambda u, c: (ring_half(1, u), c)[1], 0)
+                wait_across(1)
+            with jax.named_scope("plain"):
+                lax.fori_loop(0, near_half, plain_step, 0)
+
+        return carry
+
+    lax.fori_loop(0, 2, sequences, 0)
     with jax.named_scope("far"):
         lax.fori_loop(0, near_half, far_step, 0)
-    with jax.named_scope("plain"):
-        lax.fori_loop(0, near_half, plain_step, 0)
     with jax.named_scope("joined"):
         lax.fori_loop(0, near_half, joined_step, 0)
     with jax.named_scope("own"):
@@ -516,8 +573,9 @@
         remote(send_far.at[way], send_far.at[way], far_send.at[way], far_recv.at[way, 0], tp=other).wait_send()
         remote(send_near.at[way], send_near.at[way], near_send.at[way], near_recv.at[way, 0], tp=other).wait_send()
     remote(aux.at[t], aux.at[t], aux_send, aux_recv, tp=other).wait_send()
-    remote(kv_src, kv_src, halo_send.at[0], halo_recv.at[0], tp=other).wait_send()
-    remote(gated_src, gated_src, halo_send.at[1], halo_recv.at[1], tp=other).wait_send()
+    for turn in range(2):
+        for n, src, dst in halo_copies(2 * turn, turn):
+            remote(src, src, halo_send.at[n], halo_recv.at[n], tp=other).wait_send()
 
 
 def local(
@@ -544,12 +602,27 @@
     inside = 4 * quarter + kvw
     vmem = pl.BlockSpec(memory_space=pltpu.VMEM)
     dma = pltpu.SemaphoreType.DMA
+    arrays = (
+        tokens[0],
+        norm_gain[None],
+        w_query,
+        w_conv_in,
+        w_cgate,
+        w_bgate,
+        w_key,
+        w_value,
+        conv_taps,
+        sink_logits[None],
+        conv_out_weight.T,
+        attn_out_weight.T,
+    )
     out = pl.pallas_call(
         functools.partial(layer_kernel, ns, nf),
         out_shape=jax.ShapeDtypeStruct((rows, width), BF16),
-        in_specs=[vmem] * 12,
+        in_specs=[pl.BlockSpec(memory_space=pltpu.HBM)] * 12,
         out_specs=vmem,
         scratch_shapes=[
+            *(pltpu.VMEM(a.shape, a.dtype) for a in arrays),
             pltpu.VMEM((nf, rows, width), BF16),
             pltpu.VMEM((ns, 2, 2 * rb, inside), BF16),
             pltpu.VMEM((ns, 2, 2 * rb, 2 * quarter), BF16),
@@ -577,31 +650,19 @@
             dma((2, 3)),
             dma,
             dma,
-            dma((2,)),
-            dma((2,)),
+            dma((4,)),
+            dma((4,)),
             dma((2,)),
             dma((2, count // 2)),
             dma((2,)),
             dma((2, count)),
+            dma((len(arrays),)),
         ],
         compiler_params=pltpu.CompilerParams(
             collective_id=0, has_side_effects=True, vmem_limit_bytes=62 * 1024 * 1024
         ),
         name="layer",
-    )(
-        tokens[0],
-        norm_gain[None],
-        w_query,
-        w_conv_in,
-        w_cgate,
-        w_bgate,
-        w_key,
-        w_value,
-        conv_taps,
-        sink_logits[None],
-        conv_out_weight.T,
-        attn_out_weight.T,
-    )
+    )(*arrays)
     return out[None]
 
 

time: 150 us -> 135 us (0.900)
  Pallas kernels: 148 us -> 132 us
    pallas_call x1, Pallas kernels: 148 us -> 132 us  [local(): pl.pallas_call(functools.partial(layer_kernel, ns, nf), out_shape=jax.Sha...]
where the time goes in v3:
time: 135 us; the launch traced here: 134 us
  Pallas kernels  132 us (98%)
  local copies, waits for them, and re-layouts  2.3 us (2%)
    pallas_call x1, Pallas kernels, local(): pl.pallas_call(functools.partial(layer_kernel, ns, nf), out_shape=jax.Sha...  132 us

profile of v3, /device:TPU:33, one launch (start us, length us, event | category | flops | bytes accessed | tf_op | source)
XLA Modules:
  0.0 134.2 jit_solution(11082071029495107679)
XLA Ops:
  0.0 131.9 %layer.1 = bf16[256,2048]{1,0:T(8,128)(2,1)} custom-call(bf16[256,2048]{1,0:T(8,128)(2,1)} %bitcast.7, f32[1,2048]{1,0:T(1,128)} %bitcast.10, bf16[32,1024]{1,0:T(8,128)(2,1)} %refs_2_.1, bf16[32,1024]{1,0:T(8,128)(2,1)} %refs_3_.1, bf16[32,1024]{1,0:T(8,128)(2,1)} %refs_4_.1, bf16[32,1024]{1,0:T(8,128)(2,1)} %refs_5_.1, bf16[32,128]{1,0:T(8,128)(2,1)} %refs_6_.1, ...), custom_call_target="tpu_custom_call" | custom-call | tf_op jit(solution)/shard_map/layer/pallas_call | solution.py:619
  131.9 2.3 %copy.14 = bf16[1,256,2048]{2,1,0:T(8,128)(2,1)} copy(bf16[1,256,2048]{2,1,0:T(8,128)(2,1)} %bitcast.6) | data formatting | bytes 2097152

commit v4 on v3

--- a/solution.py
+++ b/solution.py
@@ -52,6 +52,7 @@
         y_recv,
         p_send,
         p_recv,
+        out_recv,
         x_send,
         x_recv,
         aux_send,
@@ -131,14 +132,13 @@
     with jax.named_scope("meet"):
         pl.semaphore_wait(barrier, len(greeted))
 
-    y_in, y_out = 3 * quarter // 2, quarter // 2
-    z_in, z_out = y_in + quarter + kvw, 3 * quarter // 2
+    y_in, y_out = quarter + kvw, 3 * quarter // 4
+    z_in, z_out = 3 * quarter, 2 * quarter - y_out
     weights = (w_in, w_out)
     lane = pl.multiple_of
     z_span = (pl.ds(lane(odd * y_in, 128), z_in), pl.ds(lane(odd * y_out, 128), z_out))
     y_span = (pl.ds(lane(odd * z_in, 128), y_in), pl.ds(lane(odd * z_out, 128), y_out))
     y_other = (pl.ds(lane((1 - odd) * z_in, 128), y_in), pl.ds(lane((1 - odd) * z_out, 128), y_out))
-    mid = quarter // 2
 
     mine = f // 2
     first = lax.rem(f, 2)
@@ -149,16 +149,17 @@
             here = jnp.logical_and(to_f == f, mine == t)
             base = j * quarter
             if k == 0:
-                common = [(w_query, base, y_in, quarter), (kv_pack, None, y_in + quarter, kvw)]
+                at = y_in + quarter
+                common = [(w_conv_in, base, y_in, quarter), (w_cgate, base, at, z_in - at)]
                 shares = (
-                    [(w_conv_in, base, 0, quarter), (w_cgate, base, quarter, mid)],
-                    [(w_cgate, base + mid, z_in, mid), (w_bgate, base, z_in + mid, quarter)],
+                    [(w_query, base, 0, quarter), (kv_pack, None, quarter, kvw)],
+                    [(w_cgate, base + z_in - at, z_in, at + quarter - z_in), (w_bgate, base, at + quarter, quarter)],
                 )
             else:
                 common = []
                 shares = (
-                    [(conv_out, base, 0, quarter), (attn_out, base, quarter, mid)],
-                    [(conv_out, base + mid, mid, mid), (attn_out, base, quarter, quarter)],
+                    [(conv_out, base, 0, quarter), (attn_out, base, quarter, z_out - quarter)],
+                    [(conv_out, base + y_out, y_out, quarter - y_out), (attn_out, base, quarter, quarter)],
                 )
 
             def deliver(moves, here=here, to_f=to_f, j=j, k=k):
@@ -216,9 +217,12 @@
             piece, piece, z_send.at[k, way], z_recv.at[k, way, i, hop], sp=(s_next, s_prev)[way]
         )
 
-    def across(k, slot, i):
-        piece = weights[k].at[slot, t, pl.ds(i * rb, rb), z_span[k]]
-        return remote(piece, piece, p_send.at[0, k], p_recv.at[0, k], tp=other)
+    def hand_over(k, n, hop, piece):
+        recv = (p_recv.at[n], out_recv.at[n, hop])[k]
+        return remote(piece, piece, p_send.at[n, k], recv, tp=other)
+
+    def across(k, slot, i, hop):
+        hand_over(k, 0, hop, weights[k].at[slot, t, pl.ds(i * rb, rb), z_span[k]]).start()
 
     def to_pair(k, slot, i, way, hop):
         piece = weights[k].at[slot, t, pl.ds(i * rb, rb), y_span[k]]
@@ -227,7 +231,7 @@
     def from_pair(k, slot, i, way, hop):
         piece = weights[k].at[slot, t, pl.ds(i * rb, rb), y_other[k]]
         remote(piece, piece, y_send.at[k], y_recv.at[k, way, i, hop], grp=pair).wait_recv()
-        remote(piece, piece, p_send.at[1, k], p_recv.at[1, k], tp=other).start()
+        hand_over(k, 1, hop, piece).start()
 
     def launch(k):
         for i in range(2):
@@ -236,7 +240,7 @@
                     onward(k, s, i, way, 1).start()
             to_pair(k, s, i, 0, 0).start()
         for i in range(2):
-            across(k, s, i).start()
+            across(k, s, i, 0)
 
     def slot_of(way, hop):
         return lax.rem(s + ns - hop, ns) if way == 0 else lax.rem(s + hop, ns)
@@ -248,7 +252,7 @@
                 onward(k, slot, i, way, hop).wait_recv()
                 when(hop < reach[way][i], lambda: onward(k, slot, i, way, hop + 1).start())
                 to_pair(k, slot, i, way, hop).start()
-                across(k, slot, i).start()
+                across(k, slot, i, hop)
 
             when(hop <= reach[way][i], body)
 
@@ -268,7 +272,7 @@
         for i in range(2):
             pair_part(k, hop, i)
 
-    lag = 2
+    lag, out_lag = 2, 1
 
     def ring_half(k, u):
         hop = u // 2
@@ -277,33 +281,50 @@
             @pl.when(lax.rem(u, 2) == i)
             def _():
                 pl.when(jnp.logical_and(hop >= 1, hop <= last))(lambda: ring_part(k, hop, i))
-                pl.when(jnp.logical_and(hop >= lag, hop <= last + lag))(lambda: pair_part(k, hop - lag, i))
+                pl.when(jnp.logical_and(hop >= out_lag, hop <= last + out_lag))(lambda: pair_part(k, hop - out_lag, i))
 
     last = ns // 2
 
-    def wait_across(k):
+    def wait_across():
         for n, span in ((0, z_span), (1, y_other)):
-            piece = weights[k].at[:, other, :, span[k]]
-            remote(piece, piece, p_send.at[n, k], p_recv.at[n, k], tp=other).wait_recv()
+            hand_over(0, n, 0, w_in.at[:, other, :, span[0]]).wait_recv()
+
+    def ready(hop):
+        chips_there = 1 if hop in (0, last) else 2
+        for n, span in ((0, z_span), (1, y_other)):
+            hand_over(1, n, hop, w_out.at[pl.ds(0, chips_there), other, :, span[1]]).wait_recv()
 
     with jax.named_scope("first_wait"):
         wait_first(0)
     launch(0)
+    first_exchange(1)
     halves = (pl.ds(0, half), pl.ds(half, half))
     for which in (0, 1):
         for way, part, to in ((0, which, f_next), (1, 1 - which, f_prev)):
             ref = x_all.at[mine_seat, halves[part]]
             remote(ref, ref, x_send.at[way], x_recv.at[way, part], fs=to).start()
-    first_exchange(1)
     early = max(1, ns // 4)
-    start_out = max(last - 2, early)
-    ahead = min(1, start_out - 1)
+    start_out = max(last - 5, 1)
+    ahead = min(1, start_out)
     resume = 2 * (last - start_out + ahead + 1)
+
+    def both_rings(hop):
+        ring_step(0, hop)
+        if hop >= lag:
+            pair_step(0, hop - lag)
+        if hop == start_out:
+            wait_first(1)
+            launch(1)
+        second_ring(hop - start_out)
+
+    def second_ring(hop):
+        if hop >= 1:
+            ring_step(1, hop)
+            pair_step(1, hop - out_lag)
+
     with jax.named_scope("ring0_early"):
         for hop in range(1, early):
-            ring_step(0, hop)
-            if hop >= 2:
-                pair_step(0, hop - 2)
+            both_rings(hop)
 
     def x_block(which, part, way, kind):
         ref = x_all.at[which, halves[part]]
@@ -316,28 +337,19 @@
         x_block(next_seat, 1, 1, 2).start()
     with jax.named_scope("ring0_late"):
         for hop in range(early, last + 1):
-            ring_step(0, hop)
-            if hop >= 2:
-                pair_step(0, hop - 2)
-            if hop == start_out:
-                wait_first(1)
-                launch(1)
-            if hop > start_out:
-                ring_step(1, hop - start_out)
+            both_rings(hop)
     with jax.named_scope("pair_late"):
-        for hop in range(max(last - 1, 0), last + 1):
+        for hop in range(max(last + 1 - lag, 0), last + 1):
             pair_step(0, hop)
-            if 1 <= hop + ahead - last <= ahead:
-                ring_step(1, last - start_out + hop + ahead - last)
-        for hop in range(0, max(resume // 2 - lag, 0)):
-            pair_step(1, hop)
+            if last - hop < ahead:
+                second_ring(last - start_out + ahead - (last - hop))
     with jax.named_scope("rows_wait"):
         x_block(prev_seat, 1, 0, 1).wait_recv()
         x_block(next_seat, 0, 1, 0).wait_recv()
         x_block(far_seat, 0, 0, 2).wait_recv()
         x_block(far_seat, 1, 1, 2).wait_recv()
     with jax.named_scope("across0"):
-        wait_across(0)
+        wait_across()
     remote(aux.at[other], aux.at[other], aux_send, aux_recv, tp=other).wait_recv()
 
     def project(base, column, size):
@@ -370,7 +382,7 @@
 
     def gate(q, carry):
         for n in range(per):
-            product = proj[n, q].astype(F32) * proj[(2, 5)[n], q].astype(F32)
+            product = proj[per + n, q].astype(F32) * proj[2 * per + n, q].astype(F32)
             gated[q, 16:, pl.ds(n * TILE, TILE)] = product.astype(BF16)
         return carry
 
@@ -401,7 +413,7 @@
         values = jnp.transpose(values).astype(BF16)
         scores = []
         for duo in range(duos):
-            n, column = 3 + duo * 2 * HEAD // TILE, duo * 2 * HEAD % TILE
+            n, column = duo * 2 * HEAD // TILE, duo * 2 * HEAD % TILE
             scores.append(rows_dot(keys, proj[n, q, begin : begin + WINDOW, column : column + 2 * HEAD]))
         probs = []
         for duo in range(duos):
@@ -433,15 +445,19 @@
                 + pltpu.roll(wide, 1, 0)[16:] * taps[1:2]
                 + wide[16:] * taps[2:3]
             )
-            acts[q, :, span] = (proj[6 + n, q].astype(F32) * total).astype(BF16)
+            acts[q, :, span] = (proj[3 * per + n, q].astype(F32) * total).astype(BF16)
         return carry
 
     count = width // TILE
     near_half = count // 2
     chips = TILE // (2 * 2 * rb)
 
-    def partial(q, n):
-        w = w_out[pl.ds(n * chips, chips)].reshape(TILE, 2 * quarter)
+    def place(k):
+        away = (k + 1) // 2 * (2 * lax.rem(k, 2) - 1) * (2 * lax.rem(s, 2) - 1)
+        return lax.rem(s // chips + away + count, count)
+
+    def partial(q, k):
+        w = w_out[pl.ds(place(k) * chips, chips)].reshape(TILE, 2 * quarter)
         return rows_dot(acts[q], w)
 
     ways = (f_next, f_prev)
@@ -455,55 +471,57 @@
         )
 
     def far_step(n, carry):
-        send_far[0, n] = partial(far_seat, n).astype(BF16)
-        send_far[1, n] = partial(far_seat, n + near_half).astype(BF16)
-        far_copy(0, n).start()
-        far_copy(1, n).start()
+        parts = [partial(far_seat, 2 * n + way).astype(BF16) for way in range(2)]
+        for way in range(2):
+            send_far[way, n] = parts[way]
+        for way in range(2):
+            far_copy(way, n).start()
         return carry
 
     def plain_step(n, carry):
-        send_near[0, n + near_half] = partial(next_seat, n + near_half).astype(BF16)
-        send_near[1, n] = partial(prev_seat, n).astype(BF16)
-        near_copy(0, n + near_half).start()
-        near_copy(1, n).start()
+        parts = [partial(q, 2 * n + 1 - way).astype(BF16) for way, q in ((0, next_seat), (1, prev_seat))]
+        for way in range(2):
+            send_near[way, 2 * n + 1 - way] = parts[way]
+        for way in range(2):
+            near_copy(way, 2 * n + 1 - way).start()
         return carry
 
     def joined_step(n, carry):
-        right, left = partial(next_seat, n), partial(prev_seat, n + near_half)
-        far_copy(0, n).wait_recv()
-        far_copy(1, n).wait_recv()
-        send_near[0, n] = (right + recv_far[0, n].astype(F32)).astype(BF16)
-        send_near[1, n + near_half] = (left + recv_far[1, n].astype(F32)).astype(BF16)
-        near_copy(0, n).start()
-        near_copy(1, n + near_half).start()
+        parts = [partial(q, 2 * n + way) for way, q in ((0, next_seat), (1, prev_seat))]
+        for way in range(2):
+            far_copy(way, n).wait_recv()
+        for way in range(2):
+            send_near[way, 2 * n + way] = (parts[way] + recv_far[way, n].astype(F32)).astype(BF16)
+        for way in range(2):
+            near_copy(way, 2 * n + way).start()
         return carry
 
-    def own_step(n, carry):
-        own_sum[n] = partial(mine_seat, n)
+    def own_step(k, carry):
+        own_sum[k] = partial(mine_seat, k)
         return carry
 
     def sequences(turn, carry):
         base = lax.rem(f + 1 + turn, 2) * 2
         kv_halo, gated_halo = halo_copies(base, turn)
-        count_from = resume + turn * 4 * (last + lag)
 
         def projection(n, inner):
-            ring_half(1, count_from + n)
+            pl.when(jnp.logical_and(turn == 0, lax.rem(n, 2) == 0))(lambda: ring_half(1, resume + n // 2))
             pl.when(n == 1)(lambda: send_halo(*kv_halo))
-            column = pl.multiple_of(n * TILE + n // 5 * kvw, 128)
+            column = pl.multiple_of(n * TILE + (n + tiles - per) // tiles * kvw, 128)
             proj[n, pl.ds(base, 2)] = project(base, column, TILE).reshape(2, rows, TILE)
             return inner
 
         def attend(r, inner):
             for b in range(blocks):
-                ring_half(1, count_from + tiles + r * blocks + b)
+                if b == 0:
+                    pl.when(turn == 0)(lambda: ring_half(1, resume + tiles // 2 + r))
                 attend_block(base + r, b)
                 if b == 0:
                     pl.when(r == 0)(lambda: send_halo(*gated_halo))
             return inner
 
         with jax.named_scope("project_kv"):
-            kv_rows[pl.ds(base, 2), WINDOW:, :] = project(base, y_in + quarter, kvw).reshape(2, rows, kvw)
+            kv_rows[pl.ds(base, 2), WINDOW:, :] = project(base, quarter, kvw).reshape(2, rows, kvw)
         with jax.named_scope("projections"):
             lax.fori_loop(0, tiles, projection, 0)
         with jax.named_scope("gates"):
@@ -525,8 +543,10 @@
         @pl.when(turn == 0)
         def _():
             with jax.named_scope("across1"):
-                lax.fori_loop(resume + tiles + 2 * blocks, 2 * (last + lag) + 2, lambda u, c: (ring_half(1, u), c)[1], 0)
-                wait_across(1)
+                rest = resume + tiles // 2 + 2
+                lax.fori_loop(rest, max(rest, 2 * (last + out_lag) + 2), lambda u, c: (ring_half(1, u), c)[1], 0)
+                for hop in range(last + 1):
+                    ready(hop)
             with jax.named_scope("plain"):
                 lax.fori_loop(0, near_half, plain_step, 0)
 
@@ -541,14 +561,14 @@
         lax.fori_loop(0, count, own_step, 0)
     with jax.named_scope("finish"):
         for n in range(near_half):
-            for way, tile in ((0, n + near_half), (1, n)):
-                near_copy(way, tile).wait_recv()
+            for way in range(2):
+                near_copy(way, 2 * n + 1 - way).wait_recv()
         for n in range(near_half):
-            for way, tile in ((0, n), (1, n + near_half)):
-                near_copy(way, tile).wait_recv()
-            for tile in (n, n + near_half):
-                total = own_sum[tile] + recv_near[0, tile].astype(F32) + recv_near[1, tile].astype(F32)
-                out[:, tile * TILE : (tile + 1) * TILE] = total.astype(BF16)
+            for way in range(2):
+                near_copy(way, 2 * n + way).wait_recv()
+            for k in (2 * n, 2 * n + 1):
+                total = own_sum[k] + recv_near[0, k].astype(F32) + recv_near[1, k].astype(F32)
+                out[:, pl.ds(pl.multiple_of(place(k) * TILE, TILE), TILE)] = total.astype(BF16)
 
     for k in range(2):
         for j in range(2):
@@ -564,7 +584,7 @@
             remote(pieces, pieces, z_send.at[k, way], z_recv.at[k, way, 0, 0], tp=other).wait_send()
         for n, span in ((0, z_span), (1, y_other)):
             piece = weights[k].at[:, t, :, span[k]]
-            remote(piece, piece, p_send.at[n, k], p_recv.at[n, k], tp=other).wait_send()
+            hand_over(k, n, 0, piece).wait_send()
         piece = weights[k].at[:, t, :, y_span[k]]
         remote(piece, piece, y_send.at[k], y_recv.at[k, 0, 0, 0], tp=other).wait_send()
     for way in range(2):
@@ -645,7 +665,8 @@
             dma((2,)),
             dma((2, 2, 2, ns // 2 + 1)),
             dma((2, 2)),
-            dma((2, 2)),
+            dma((2,)),
+            dma((2, ns // 2 + 1)),
             dma((2,)),
             dma((2, 3)),
             dma,
@@ -659,10 +680,10 @@
             dma((len(arrays),)),
         ],
         compiler_params=pltpu.CompilerParams(
-            collective_id=0, has_side_effects=True, vmem_limit_bytes=62 * 1024 * 1024
+            collective_id=0, has_side_effects=True, vmem_limit_bytes=50 * 1024 * 1024
         ),
         name="layer",
-    )(*arrays)
+    )(*(pltpu.with_memory_space_constraint(a, pltpu.HBM) for a in arrays))
     return out[None]
 
 

time: 135 us -> 129 us (0.956)
  Pallas kernels: 132 us -> 128 us
    pallas_call x1, Pallas kernels: 132 us -> 128 us  [local(): pl.pallas_call(functools.partial(layer_kernel, ns, nf), out_shape=jax.Sha...]
where the time goes in v4:
time: 129 us
  Pallas kernels  128 us (99%)
    pallas_call x1, Pallas kernels, local(): pl.pallas_call(functools.partial(layer_kernel, ns, nf), out_shape=jax.Sha...  128 us

profile of v4, /device:TPU:33, one launch (start us, length us, event | category | flops | bytes accessed | tf_op | source)
XLA Modules:
  0.0 128.6 jit_solution(6014704238488343831)
XLA Ops:
  0.0 127.6 %layer.1 = bf16[256,2048]{1,0:T(8,128)(2,1)S(1)} custom-call(bf16[256,2048]{1,0:T(8,128)(2,1)} %bitcast.7, f32[1,2048]{1,0:T(1,128)} %bitcast.10, bf16[32,1024]{1,0:T(8,128)(2,1)} %refs_2_.1, bf16[32,1024]{1,0:T(8,128)(2,1)} %refs_3_.1, bf16[32,1024]{1,0:T(8,128)(2,1)} %refs_4_.1, bf16[32,1024]{1,0:T(8,128)(2,1)} %refs_5_.1, bf16[32,128]{1,0:T(8,128)(2,1)} %refs_6_.1, ...), custom_call_target="tpu_custom_call" | custom-call | tf_op jit(solution)/shard_map/layer/pallas_call | solution.py:639
  127.6 1.0 copy.14

commit v5 on v4

--- a/solution.py
+++ b/solution.py
@@ -44,6 +44,8 @@
         send_near,
         recv_near,
         own_sum,
+        started,
+        started_kv,
         first_send,
         first_recv,
         z_send,
@@ -52,7 +54,6 @@
         y_recv,
         p_send,
         p_recv,
-        out_recv,
         x_send,
         x_recv,
         aux_send,
@@ -166,7 +167,7 @@
                 def ends(move):
                     ref, start, column, size = move
                     src = ref.at[j] if start is None else ref.at[:, pl.ds(start, size)]
-                    return src, weights[k].at[s, mine, slot_rows, pl.ds(column, size)]
+                    return src, weights[k].at[(0, s)[k], mine, slot_rows, pl.ds(column, size)]
 
                 @pl.when(jnp.logical_not(here))
                 def _():
@@ -190,11 +191,17 @@
         loads[0].wait()
         step_rows = 32
 
+        chunk = width // ns
+
         def norm(r, carry):
             span = pl.ds(pl.multiple_of(r * step_rows, step_rows), step_rows)
             wide = tokens[span, :].astype(F32)
             scale = lax.rsqrt(jnp.mean(wide * wide, axis=-1, keepdims=True) + EPSILON)
-            x_all[mine_seat, span, :] = (wide * scale * gain[...]).astype(BF16)
+            for p in range(ns):
+                away = p // 2 if p % 2 == 0 else ns - (p + 1) // 2
+                block = pl.ds(pl.multiple_of(lax.rem(s + away, ns) * chunk, chunk), chunk)
+                part = tokens[span, block].astype(F32) * scale * gain[:, block]
+                x_all[mine_seat, span, p * chunk : (p + 1) * chunk] = part.astype(BF16)
             return carry
 
         lax.fori_loop(0, rows // step_rows, norm, 0)
@@ -206,30 +213,43 @@
 
             @pl.when(jnp.logical_not(local))
             def _():
-                piece = weights[k].at[s, t, pl.ds(i * rb, rb), z_span[k]]
+                piece = weights[k].at[(0, s)[k], t, pl.ds(i * rb, rb), z_span[k]]
                 remote(piece, piece, first_send.at[k, 0], first_recv.at[k, i], tp=other).wait_recv()
 
     reach = ((ns // 2, ns // 2 - 1), (ns // 2 - 1, ns // 2))
 
-    def onward(k, slot, i, way, hop):
-        piece = weights[k].at[slot, t, pl.ds(i * rb, rb), z_span[k]]
-        return remote(
-            piece, piece, z_send.at[k, way], z_recv.at[k, way, i, hop], sp=(s_next, s_prev)[way]
-        )
+    def slot_of(way, hop):
+        return lax.rem(s + ns - hop, ns) if way == 0 else lax.rem(s + hop, ns)
+
+    def spot(k, way, hop):
+        if k == 1:
+            return slot_of(way, hop)
+        return min(max(2 * hop - 1 + way, 0), ns - 1)
+
+    def piece_of(k, way, hop, i, span):
+        return weights[k].at[spot(k, way, hop), t, pl.ds(i * rb, rb), span[k]]
+
+    def onward(k, i, way, hop):
+        src = piece_of(k, way, hop - 1, i, z_span)
+        dst = src if k == 1 else piece_of(k, way, hop, i, z_span)
+        return remote(src, dst, z_send.at[k, way], z_recv.at[k, way, i, hop], sp=(s_next, s_prev)[way])
+
+    def arrival(k, i, way, hop):
+        piece = piece_of(k, way, hop, i, z_span)
+        return remote(piece, piece, z_send.at[k, way], z_recv.at[k, way, i, hop], sp=(s_next, s_prev)[way])
 
     def hand_over(k, n, hop, piece):
-        recv = (p_recv.at[n], out_recv.at[n, hop])[k]
-        return remote(piece, piece, p_send.at[n, k], recv, tp=other)
-
-    def across(k, slot, i, hop):
-        hand_over(k, 0, hop, weights[k].at[slot, t, pl.ds(i * rb, rb), z_span[k]]).start()
-
-    def to_pair(k, slot, i, way, hop):
-        piece = weights[k].at[slot, t, pl.ds(i * rb, rb), y_span[k]]
+        return remote(piece, piece, p_send.at[k, n], p_recv.at[k, n, hop], tp=other)
+
+    def across(k, i, way, hop):
+        hand_over(k, 0, hop, piece_of(k, way, hop, i, z_span)).start()
+
+    def to_pair(k, i, way, hop):
+        piece = piece_of(k, way, hop, i, y_span)
         return remote(piece, piece, y_send.at[k], y_recv.at[k, way, i, hop], grp=pair)
 
-    def from_pair(k, slot, i, way, hop):
-        piece = weights[k].at[slot, t, pl.ds(i * rb, rb), y_other[k]]
+    def from_pair(k, i, way, hop):
+        piece = piece_of(k, way, hop, i, y_other)
         remote(piece, piece, y_send.at[k], y_recv.at[k, way, i, hop], grp=pair).wait_recv()
         hand_over(k, 1, hop, piece).start()
 
@@ -237,28 +257,25 @@
         for i in range(2):
             for way in range(2):
                 if reach[way][i] >= 1:
-                    onward(k, s, i, way, 1).start()
-            to_pair(k, s, i, 0, 0).start()
+                    onward(k, i, way, 1).start()
+            to_pair(k, i, 0, 0).start()
         for i in range(2):
-            across(k, s, i, 0)
-
-    def slot_of(way, hop):
-        return lax.rem(s + ns - hop, ns) if way == 0 else lax.rem(s + hop, ns)
+            across(k, i, 0, 0)
 
     def ring_part(k, hop, i):
         for way in range(2):
 
-            def body(slot=slot_of(way, hop), way=way):
-                onward(k, slot, i, way, hop).wait_recv()
-                when(hop < reach[way][i], lambda: onward(k, slot, i, way, hop + 1).start())
-                to_pair(k, slot, i, way, hop).start()
-                across(k, slot, i, hop)
+            def body(way=way):
+                arrival(k, i, way, hop).wait_recv()
+                when(hop < reach[way][i], lambda: onward(k, i, way, hop + 1).start())
+                to_pair(k, i, way, hop).start()
+                across(k, i, way, hop)
 
             when(hop <= reach[way][i], body)
 
     def pair_part(k, hop, i):
         for way in range(2):
-            body = functools.partial(from_pair, k, slot_of(way, hop), i, way, hop)
+            body = functools.partial(from_pair, k, i, way, hop)
             if isinstance(hop, int):
                 when(way <= hop <= reach[way][i], body)
             else:
@@ -285,14 +302,10 @@
 
     last = ns // 2
 
-    def wait_across():
-        for n, span in ((0, z_span), (1, y_other)):
-            hand_over(0, n, 0, w_in.at[:, other, :, span[0]]).wait_recv()
-
-    def ready(hop):
+    def ready(k, hop):
         chips_there = 1 if hop in (0, last) else 2
         for n, span in ((0, z_span), (1, y_other)):
-            hand_over(1, n, hop, w_out.at[pl.ds(0, chips_there), other, :, span[1]]).wait_recv()
+            hand_over(k, n, hop, weights[k].at[pl.ds(0, chips_there), other, :, span[k]]).wait_recv()
 
     with jax.named_scope("first_wait"):
         wait_first(0)
@@ -304,12 +317,39 @@
             ref = x_all.at[mine_seat, halves[part]]
             remote(ref, ref, x_send.at[way], x_recv.at[way, part], fs=to).start()
     early = max(1, ns // 4)
-    start_out = max(last - 5, 1)
+    soon = max(last - 4, 0)
+    soon_blocks = min(2 * soon + 1, ns - 1)
+    tiles = 4 * quarter // TILE
+    near_base = lax.rem(f + 1, 2) * 2
+
+    def column_of(n):
+        return pl.multiple_of(n * TILE + (n + tiles - tiles // 4) // tiles * kvw, 128)
+
+    def product(base, column, size, lo, hi):
+        w = w_in[lo:hi, :, :, pl.ds(column, size)].reshape((hi - lo) * chunk, size)
+        a = x_all[pl.ds(base, 2), :, lo * chunk : hi * chunk].reshape(2 * rows, (hi - lo) * chunk)
+        return jnp.dot(a, w, preferred_element_type=F32)
+
+    def begin_tile(base, n):
+        started[n] = product(base, column_of(n), TILE, 0, soon_blocks)
+
+    def begin_kv(base):
+        started_kv[...] = product(base, quarter, kvw, 0, soon_blocks)
+
+    def begin(which):
+        per_site = tiles // 2 - 1
+        lo, hi = which * per_site, min((which + 1) * per_site, tiles)
+        with jax.named_scope("begin"):
+            lax.fori_loop(lo, hi, lambda n, c: (begin_tile(near_base, n), c)[1], 0)
+            if hi == tiles:
+                begin_kv(near_base)
+    start_out = max(last - 6, 1)
     ahead = min(1, start_out)
     resume = 2 * (last - start_out + ahead + 1)
 
-    def both_rings(hop):
-        ring_step(0, hop)
+    def both_rings(hop, whole=True):
+        if whole:
+            ring_step(0, hop)
         if hop >= lag:
             pair_step(0, hop - lag)
         if hop == start_out:
@@ -336,26 +376,31 @@
         x_block(next_seat, 1, 1, 1).wait_recv()
         x_block(next_seat, 1, 1, 2).start()
     with jax.named_scope("ring0_late"):
-        for hop in range(early, last + 1):
+        for hop in range(early, last - 1):
             both_rings(hop)
+        for hop in range(soon + 1):
+            ready(0, hop)
+        x_block(prev_seat, 1, 0, 1).wait_recv()
+        x_block(next_seat, 0, 1, 0).wait_recv()
+        ring_step(0, last - 1)
+        begin(0)
+        both_rings(last - 1, False)
+        begin(1)
+        ring_step(0, last)
+        begin(2)
+        both_rings(last, False)
     with jax.named_scope("pair_late"):
         for hop in range(max(last + 1 - lag, 0), last + 1):
             pair_step(0, hop)
             if last - hop < ahead:
                 second_ring(last - start_out + ahead - (last - hop))
     with jax.named_scope("rows_wait"):
-        x_block(prev_seat, 1, 0, 1).wait_recv()
-        x_block(next_seat, 0, 1, 0).wait_recv()
         x_block(far_seat, 0, 0, 2).wait_recv()
         x_block(far_seat, 1, 1, 2).wait_recv()
     with jax.named_scope("across0"):
-        wait_across()
+        for hop in range(soon + 1, last + 1):
+            ready(0, hop)
     remote(aux.at[other], aux.at[other], aux_send, aux_recv, tp=other).wait_recv()
-
-    def project(base, column, size):
-        w = w_in[:, :, :, pl.ds(column, size)].reshape(width, size)
-        a = x_all[pl.ds(base, 2)].reshape(2 * rows, width)
-        return jnp.dot(a, w, preferred_element_type=F32).astype(BF16)
 
     def halo_refs(ref, base, tail):
         here = ref.at[pl.ds(base, 2)]
@@ -375,8 +420,6 @@
 
     def wait_halo(n, src, dst):
         remote(dst, dst, halo_send.at[n], halo_recv.at[n], tp=other).wait_recv()
-
-    tiles = 4 * quarter // TILE
 
     per = quarter // TILE
 
@@ -505,27 +548,42 @@
         kv_halo, gated_halo = halo_copies(base, turn)
 
         def projection(n, inner):
-            pl.when(jnp.logical_and(turn == 0, lax.rem(n, 2) == 0))(lambda: ring_half(1, resume + n // 2))
+            pl.when(jnp.logical_and(jnp.logical_and(turn == 0, n >= 2), lax.rem(n, 2) == 0))(
+                lambda: ring_half(1, resume + n // 2 - 1)
+            )
             pl.when(n == 1)(lambda: send_halo(*kv_halo))
-            column = pl.multiple_of(n * TILE + (n + tiles - per) // tiles * kvw, 128)
-            proj[n, pl.ds(base, 2)] = project(base, column, TILE).reshape(2, rows, TILE)
+            m = lax.rem(n + per, 3 * per) + n // (3 * per) * (2 * per)
+
+            @pl.when(turn == 0)
+            def _():
+                done = started[m] + product(base, column_of(m), TILE, soon_blocks, ns)
+                proj[m, pl.ds(base, 2)] = done.astype(BF16).reshape(2, rows, TILE)
+
+            @pl.when(turn == 1)
+            def _():
+                done = product(base, column_of(m), TILE, 0, ns)
+                proj[m, pl.ds(base, 2)] = done.astype(BF16).reshape(2, rows, TILE)
+
+            @pl.when(n == 2 * per - 1)
+            def _():
+                lax.fori_loop(base, base + 2, gate, 0)
+
+            pl.when(n == 2 * per + 1)(lambda: send_halo(*gated_halo))
             return inner
 
         def attend(r, inner):
             for b in range(blocks):
                 if b == 0:
-                    pl.when(turn == 0)(lambda: ring_half(1, resume + tiles // 2 + r))
+                    pl.when(jnp.logical_and(turn == 0, r == 0))(lambda: ring_half(1, resume + tiles // 2 - 1))
                 attend_block(base + r, b)
-                if b == 0:
-                    pl.when(r == 0)(lambda: send_halo(*gated_halo))
             return inner
 
         with jax.named_scope("project_kv"):
-            kv_rows[pl.ds(base, 2), WINDOW:, :] = project(base, quarter, kvw).reshape(2, rows, kvw)
+            pl.when(turn == 1)(lambda: begin_kv(base))
+            done = started_kv[...] + product(base, quarter, kvw, soon_blocks, ns)
+            kv_rows[pl.ds(base, 2), WINDOW:, :] = done.astype(BF16).reshape(2, rows, kvw)
         with jax.named_scope("projections"):
             lax.fori_loop(0, tiles, projection, 0)
-        with jax.named_scope("gates"):
-            lax.fori_loop(base, base + 2, gate, 0)
         with jax.named_scope("halo_wait"):
             wait_halo(*kv_halo)
         with jax.named_scope("attention"):
@@ -543,10 +601,10 @@
         @pl.when(turn == 0)
         def _():
             with jax.named_scope("across1"):
-                rest = resume + tiles // 2 + 2
+                rest = resume + tiles // 2
                 lax.fori_loop(rest, max(rest, 2 * (last + out_lag) + 2), lambda u, c: (ring_half(1, u), c)[1], 0)
                 for hop in range(last + 1):
-                    ready(hop)
+                    ready(1, hop)
             with jax.named_scope("plain"):
                 lax.fori_loop(0, near_half, plain_step, 0)
 
@@ -658,6 +716,8 @@
             pltpu.VMEM((2, count, rows, TILE), BF16),
             pltpu.VMEM((2, count, rows, TILE), BF16),
             pltpu.VMEM((count, rows, TILE), F32),
+            pltpu.VMEM((4 * quarter // TILE, 2 * rows, TILE), F32),
+            pltpu.VMEM((2 * rows, kvw), F32),
             dma((2, 2)),
             dma((2, 2)),
             dma((2, 2)),
@@ -665,8 +725,7 @@
             dma((2,)),
             dma((2, 2, 2, ns // 2 + 1)),
             dma((2, 2)),
-            dma((2,)),
-            dma((2, ns // 2 + 1)),
+            dma((2, 2, ns // 2 + 1)),
             dma((2,)),
             dma((2, 3)),
             dma,

time: 129 us -> 127 us (0.984)
  Pallas kernels: 128 us -> 125 us
    pallas_call x1, Pallas kernels: 128 us -> 125 us  [local(): pl.pallas_call(functools.partial(layer_kernel, ns, nf), out_shape=jax.Sha...]
where the time goes in v5:
time: 127 us; the launch traced here: 126 us
  Pallas kernels  125 us (98%)
    pallas_call x1, Pallas kernels, local(): pl.pallas_call(functools.partial(layer_kernel, ns, nf), out_shape=jax.Sha...  125 us

profile of v5, /device:TPU:33, one launch (start us, length us, event | category | flops | bytes accessed | tf_op | source)
XLA Modules:
  0.0 126.3 jit_solution(10689471170784704884)
XLA Ops:
  0.0 125.3 %layer.1 = bf16[256,2048]{1,0:T(8,128)(2,1)S(1)} custom-call(bf16[256,2048]{1,0:T(8,128)(2,1)} %bitcast.7, f32[1,2048]{1,0:T(1,128)} %bitcast.10, bf16[32,1024]{1,0:T(8,128)(2,1)} %refs_2_.1, bf16[32,1024]{1,0:T(8,128)(2,1)} %refs_3_.1, bf16[32,1024]{1,0:T(8,128)(2,1)} %refs_4_.1, bf16[32,1024]{1,0:T(8,128)(2,1)} %refs_5_.1, bf16[32,128]{1,0:T(8,128)(2,1)} %refs_6_.1, ...), custom_call_target="tpu_custom_call" | custom-call | tf_op jit(solution)/shard_map/layer/pallas_call | solution.py:697
  125.3 1.0 copy.14

commit v6 on v5

--- a/solution.py
+++ b/solution.py
@@ -207,14 +207,13 @@
         lax.fori_loop(0, rows // step_rows, norm, 0)
     remote(aux.at[t], aux.at[t], aux_send, aux_recv, tp=other).start()
 
-    def wait_first(k):
-        for i in range(2):
-            local = jnp.logical_and(t == f // 2, f == 2 * t + i)
-
-            @pl.when(jnp.logical_not(local))
-            def _():
-                piece = weights[k].at[(0, s)[k], t, pl.ds(i * rb, rb), z_span[k]]
-                remote(piece, piece, first_send.at[k, 0], first_recv.at[k, i], tp=other).wait_recv()
+    def wait_first(k, i):
+        local = jnp.logical_and(t == f // 2, f == 2 * t + i)
+
+        @pl.when(jnp.logical_not(local))
+        def _():
+            piece = weights[k].at[(0, s)[k], t, pl.ds(i * rb, rb), z_span[k]]
+            remote(piece, piece, first_send.at[k, 0], first_recv.at[k, i], tp=other).wait_recv()
 
     reach = ((ns // 2, ns // 2 - 1), (ns // 2 - 1, ns // 2))
 
@@ -255,6 +254,7 @@
 
     def launch(k):
         for i in range(2):
+            wait_first(k, i)
             for way in range(2):
                 if reach[way][i] >= 1:
                     onward(k, i, way, 1).start()
@@ -308,8 +308,7 @@
             hand_over(k, n, hop, weights[k].at[pl.ds(0, chips_there), other, :, span[k]]).wait_recv()
 
     with jax.named_scope("first_wait"):
-        wait_first(0)
-    launch(0)
+        launch(0)
     first_exchange(1)
     halves = (pl.ds(0, half), pl.ds(half, half))
     for which in (0, 1):
@@ -353,7 +352,6 @@
         if hop >= lag:
             pair_step(0, hop - lag)
         if hop == start_out:
-            wait_first(1)
             launch(1)
         second_ring(hop - start_out)
 
@@ -628,32 +626,33 @@
                 total = own_sum[k] + recv_near[0, k].astype(F32) + recv_near[1, k].astype(F32)
                 out[:, pl.ds(pl.multiple_of(place(k) * TILE, TILE), TILE)] = total.astype(BF16)
 
-    for k in range(2):
-        for j in range(2):
-            here = jnp.logical_and(2 * t + j == f, mine == t)
-
-            @pl.when(jnp.logical_not(here))
-            def _():
-                piece = weights[k].at[s, t, pl.ds(0, rb), z_span[k]]
-                remote(piece, piece, first_send.at[k, j], first_recv.at[k, 0], tp=other).wait_send()
-
-        for way in range(2):
-            pieces = weights[k].at[pl.ds(0, ns - 1), 0, pl.ds(0, rb), z_span[k]]
-            remote(pieces, pieces, z_send.at[k, way], z_recv.at[k, way, 0, 0], tp=other).wait_send()
-        for n, span in ((0, z_span), (1, y_other)):
-            piece = weights[k].at[:, t, :, span[k]]
-            hand_over(k, n, 0, piece).wait_send()
-        piece = weights[k].at[:, t, :, y_span[k]]
-        remote(piece, piece, y_send.at[k], y_recv.at[k, 0, 0, 0], tp=other).wait_send()
-    for way in range(2):
-        ref = x_all.at[pl.ds(0, 3), halves[0]]
-        remote(ref, ref, x_send.at[way], x_recv.at[way, 0], tp=other).wait_send()
-        remote(send_far.at[way], send_far.at[way], far_send.at[way], far_recv.at[way, 0], tp=other).wait_send()
-        remote(send_near.at[way], send_near.at[way], near_send.at[way], near_recv.at[way, 0], tp=other).wait_send()
-    remote(aux.at[t], aux.at[t], aux_send, aux_recv, tp=other).wait_send()
-    for turn in range(2):
-        for n, src, dst in halo_copies(2 * turn, turn):
-            remote(src, src, halo_send.at[n], halo_recv.at[n], tp=other).wait_send()
+    with jax.named_scope("drain"):
+        for k in range(2):
+            for j in range(2):
+                here = jnp.logical_and(2 * t + j == f, mine == t)
+
+                @pl.when(jnp.logical_not(here))
+                def _():
+                    piece = weights[k].at[s, t, pl.ds(0, rb), z_span[k]]
+                    remote(piece, piece, first_send.at[k, j], first_recv.at[k, 0], tp=other).wait_send()
+
+            for way in range(2):
+                pieces = weights[k].at[pl.ds(0, ns - 1), 0, pl.ds(0, rb), z_span[k]]
+                remote(pieces, pieces, z_send.at[k, way], z_recv.at[k, way, 0, 0], tp=other).wait_send()
+            for n, span in ((0, z_span), (1, y_other)):
+                piece = weights[k].at[:, t, :, span[k]]
+                hand_over(k, n, 0, piece).wait_send()
+            piece = weights[k].at[:, t, :, y_span[k]]
+            remote(piece, piece, y_send.at[k], y_recv.at[k, 0, 0, 0], tp=other).wait_send()
+        for way in range(2):
+            ref = x_all.at[pl.ds(0, 3), halves[0]]
+            remote(ref, ref, x_send.at[way], x_recv.at[way, 0], tp=other).wait_send()
+            remote(send_far.at[way], send_far.at[way], far_send.at[way], far_recv.at[way, 0], tp=other).wait_send()
+            remote(send_near.at[way], send_near.at[way], near_send.at[way], near_recv.at[way, 0], tp=other).wait_send()
+        remote(aux.at[t], aux.at[t], aux_send, aux_recv, tp=other).wait_send()
+        for turn in range(2):
+            for n, src, dst in halo_copies(2 * turn, turn):
+                remote(src, src, halo_send.at[n], halo_recv.at[n], tp=other).wait_send()
 
 
 def local(

time: 127 us -> 127 us (level)
  no operation moved by 1% of the time
where the time goes in v6:
time: 127 us
  Pallas kernels  126 us (99%)
    pallas_call x1, Pallas kernels, local(): pl.pallas_call(functools.partial(layer_kernel, ns, nf), out_shape=jax.Sha...  126 us

profile of v6, /device:TPU:33, one launch (start us, length us, event | category | flops | bytes accessed | tf_op | source)
XLA Modules:
  0.0 126.6 jit_solution(4636409416723369195)
XLA Ops:
  0.0 125.7 %layer.1 = bf16[256,2048]{1,0:T(8,128)(2,1)S(1)} custom-call(bf16[256,2048]{1,0:T(8,128)(2,1)} %bitcast.7, f32[1,2048]{1,0:T(1,128)} %bitcast.10, bf16[32,1024]{1,0:T(8,128)(2,1)} %refs_2_.1, bf16[32,1024]{1,0:T(8,128)(2,1)} %refs_3_.1, bf16[32,1024]{1,0:T(8,128)(2,1)} %refs_4_.1, bf16[32,1024]{1,0:T(8,128)(2,1)} %refs_5_.1, bf16[32,128]{1,0:T(8,128)(2,1)} %refs_6_.1, ...), custom_call_target="tpu_custom_call" | custom-call | tf_op jit(solution)/shard_map/layer/pallas_call | solution.py:696
  125.7 1.0 copy.14
